TPU v7x, 32 devices: a whole 2x2x4 slice. The times are simulated.
32 devices in a mesh: fs: 4 (over z), tp: 4 (over y, x), rep: 2 (over core).
Axes of the slice: x: 2, y: 2, z: 4, core: 2. Of those that a mesh axis runs over, the one named last changes fastest.
Arguments:
- gate_weight: float32 [2048, 5632], P('fs', 'tp'), may hold values from -6 to 6
- gate_momentum: float32 [2048, 5632], P('fs', 'tp'), may hold values from -60 to 60
- gate_grads: float32 [2, 2048, 5632], P('rep', 'fs', 'tp'), may hold values from -3500 to 3500
- gate_rows: float32 [2048], P('fs'), may hold values from 0.3 to 3
- gate_columns: float32 [5632], P('tp'), may hold values from 0.3 to 3
- up_weight: float32 [2048, 5632], P('fs', 'tp'), may hold values from -6 to 6
- up_momentum: float32 [2048, 5632], P('fs', 'tp'), may hold values from -60 to 60
- up_grads: float32 [2, 2048, 5632], P('rep', 'fs', 'tp'), may hold values from -3500 to 3500
- up_rows: float32 [2048], P('fs'), may hold values from 0.3 to 3
- up_columns: float32 [5632], P('tp'), may hold values from 0.3 to 3
- down_weight: float32 [5632, 2048], P('fs', 'tp'), may hold values from -6 to 6
- down_momentum: float32 [5632, 2048], P('fs', 'tp'), may hold values from -60 to 60
- down_grads: float32 [2, 5632, 2048], P('rep', 'fs', 'tp'), may hold values from -3500 to 3500
- down_rows: float32 [5632], P('fs'), may hold values from 0.3 to 3
- down_columns: float32 [2048], P('tp'), may hold values from 0.3 to 3
- mixer_weight: float32 [2048, 2048], P('fs', 'tp'), may hold values from -6 to 6
- mixer_momentum: float32 [2048, 2048], P('fs', 'tp'), may hold values from -60 to 60
- mixer_grads: float32 [2, 2048, 2048], P('rep', 'fs', 'tp'), may hold values from -3500 to 3500
- mixer_rows: float32 [2048], P('fs'), may hold values from 0.3 to 3
- mixer_columns: float32 [2048], P('tp'), may hold values from 0.3 to 3
Outputs:
- gate_weight_next: float32 [2048, 5632], P('fs', 'tp')
- gate_momentum_next: float32 [2048, 5632], P('fs', 'tp')
- gate_rows_next: float32 [2048], P('fs')
- gate_columns_next: float32 [5632], P('tp')
- up_weight_next: float32 [2048, 5632], P('fs', 'tp')
- up_momentum_next: float32 [2048, 5632], P('fs', 'tp')
- up_rows_next: float32 [2048], P('fs')
- up_columns_next: float32 [5632], P('tp')
- down_weight_next: float32 [5632, 2048], P('fs', 'tp')
- down_momentum_next: float32 [5632, 2048], P('fs', 'tp')
- down_rows_next: float32 [5632], P('fs')
- down_columns_next: float32 [2048], P('tp')
- mixer_weight_next: float32 [2048, 2048], P('fs', 'tp')
- mixer_momentum_next: float32 [2048, 2048], P('fs', 'tp')
- mixer_rows_next: float32 [2048], P('fs')
- mixer_columns_next: float32 [2048], P('tp')
All inputs are finite; a program needn't handle non-finite values.
Results may differ from a plain program's by a relative error of at most 0.00002.
Values sent between devices are 32-bit elements; how exact they have to be, the bound alone decides.
No kernel may reach another device: no remote copies, remote signals or barrier semaphores. Data moves between devices by JAX's collectives and lax.ppermute only.
A program may use at most 128 MiB of HBM per device.

v0:
```python
import jax
import jax.numpy as jnp
from jax import lax
from jax.experimental import pallas as pl
from jax.experimental.pallas import tpu as pltpu
from jax.sharding import PartitionSpec as P


momentum_decay = 0.9
moment_decay = 0.95
clip_level = 0.25
step_rate = 0.1

EVERY = ("fs", "tp", "rep")
SWAP = [(0, 1), (1, 0)]
ORDER = (0, 1, 2, 3)
LANES = 128
PARTS = 2
HBM = pl.BlockSpec(memory_space=pltpu.HBM)
VMEM = pl.BlockSpec(memory_space=pltpu.VMEM)


def up_to(n, unit):
    return (n + unit - 1) // unit * unit


def struct(*shape):
    return jax.ShapeDtypeStruct(shape, jnp.float32)


def call(kernel, ins, outs, spaces, out_spaces, scratch=(), limit=4 << 20, cost=0, aliases=None):
    ins = [pltpu.with_memory_space_constraint(x, spec.memory_space) for x, spec in zip(ins, spaces)]
    placed = [spec.memory_space(out.shape, out.dtype) for out, spec in zip(outs, out_spaces)]
    return pl.pallas_call(
        kernel,
        out_shape=placed,
        in_specs=spaces,
        out_specs=out_spaces,
        scratch_shapes=scratch,
        input_output_aliases=aliases or {},
        compiler_params=pltpu.CompilerParams(vmem_limit_bytes=limit),
        cost_estimate=pl.CostEstimate(flops=cost, bytes_accessed=0, transcendentals=0),
    )(*ins)


def swap(x):
    return lax.ppermute(x, "rep", SWAP)


def copies(pairs, sem):
    started = [pltpu.make_async_copy(a, b, sem.at[n]) for n, (a, b) in enumerate(pairs)]
    for item in started:
        item.start()
    for item in started:
        item.wait()


def other_halves(arrays):
    n = len(arrays)

    def kernel(*refs):
        me = lax.axis_index("rep")
        pairs = []
        for source, target in zip(refs[:n], refs[n : 2 * n]):
            h = target.shape[0]
            pairs.append((source.at[0, pl.ds(pl.multiple_of((1 - me) * h, 8), h)], target))
        copies(pairs, refs[-1])

    outs = [struct(g.shape[1] // 2, g.shape[2]) for g in arrays]
    return call(kernel, arrays, outs, [HBM] * n, [VMEM] * n, [pltpu.SemaphoreType.DMA((n,))], cost=1 << 21)


def own_halves(arrays):
    n = len(arrays)

    def kernel(*refs):
        me = lax.axis_index("rep")
        sem = refs[-1]
        pairs = []
        for source, target in zip(refs[:n], refs[n : 2 * n]):
            h = target.shape[0]
            at = pl.ds(pl.multiple_of(me * h, 8), h)
            pairs.append((source.at[0, at] if len(source.shape) == 3 else source.at[at], target))
        copies(pairs, sem)

    outs = [struct(a.shape[-2] // 2, a.shape[-1]) for a in arrays]
    return call(kernel, arrays, outs, [HBM] * n, [VMEM] * n, [pltpu.SemaphoreType.DMA((n,))], cost=1 << 22)


class Places:
    def __init__(self, heights, widths):
        self.halves = [h // 2 for h in heights]
        self.blocks = [up_to(h, LANES) // LANES for h in self.halves]
        self.tiles = [w // LANES for w in widths]
        self.row_at = [sum(self.blocks[:k]) for k in range(4)]
        self.column_at = [sum(self.tiles[:k]) for k in range(4)]
        self.n_row = up_to(sum(self.blocks), 8)
        self.spare = sum(self.tiles)
        self.n_column = up_to(self.spare + 1, 8)


def statistics(k, places, g, m, received, packed):
    h, width = g.shape
    n_blocks, tiles = places.blocks[k], places.tiles[k]
    row_at, column_at = places.row_at[k], places.n_row + places.column_at[k]

    def kernel(*refs):
        g_ref, m_ref, r_ref = refs[:3]
        own_ref, out_ref, partial = refs[-3:]
        if packed is None:
            out_ref[...] = jnp.zeros_like(out_ref)

        def step(i, sums):
            rows = pl.ds(pl.multiple_of(i * 8, 8), 8)
            sums = list(sums)
            by_row = None
            for j in range(tiles):
                at = (rows, pl.ds(j * LANES, LANES))
                grad = g_ref[at] + r_ref[at]
                own_ref[at] = momentum_decay * m_ref[at] + (1.0 - momentum_decay) * grad
                square = grad * grad
                sums[j] = sums[j] + square
                by_row = square if by_row is None else by_row + square
            partial[rows, :] = by_row
            return tuple(sums)

        zero = jnp.zeros((8, LANES), jnp.float32)
        sums = lax.fori_loop(0, h // 8, step, (zero,) * tiles, unroll=2)
        for j in range(tiles):
            out_ref[pl.ds(column_at + j, 1), :] = jnp.sum(sums[j], axis=0, keepdims=True)
        if n_blocks * LANES > h:
            partial[pl.ds(h, n_blocks * LANES - h), :] = jnp.zeros((n_blocks * LANES - h, LANES), jnp.float32)
        for b in range(n_blocks):
            turned = partial[pl.ds(b * LANES, LANES), :].T
            out_ref[pl.ds(row_at + b, 1), :] = jnp.sum(turned, axis=0, keepdims=True)

    ins = [g, m, received] + ([] if packed is None else [packed])
    return call(
        kernel,
        ins,
        [struct(h, width), struct(places.n_row + places.n_column, LANES)],
        [VMEM] * len(ins),
        [VMEM, VMEM],
        [pltpu.VMEM((n_blocks * LANES, LANES), jnp.float32)],
        cost=1 << 20,
        aliases=None if packed is None else {3: 1},
    )


def spread_rows(root, factor, n_blocks):
    for b in range(n_blocks):
        wide = jnp.broadcast_to(root[b : b + 1, :], (LANES, LANES)).T
        factor[pl.ds(b * LANES, LANES), :] = wide


def shares(places, column_count, rows_old, row_parts, packed, own, after):
    n_parts = len(row_parts)

    def old_rows(k, ref, me):
        h, n = places.halves[k], places.blocks[k]
        whole, rest = divmod(h, LANES)
        everything = ref[...]
        first = everything[:n]
        if rest:
            turned = pltpu.roll(everything, LANES - rest, 1)
            low = lax.broadcasted_iota(jnp.int32, (1, LANES), 1) < LANES - rest
            steps = []
            for i in range(n):
                here = turned[whole + i : whole + i + 1]
                after = turned[whole + i + 1 : whole + i + 2] if i < n - 1 else here
                steps.append(jnp.where(low, here, after))
            second = jnp.concatenate(steps, axis=0)
            at = lax.broadcasted_iota(jnp.int32, (n, LANES), 0) * LANES + lax.broadcasted_iota(jnp.int32, (n, LANES), 1)
            return jnp.where(at < h, jnp.where(me == 0, first, second), 0.0)
        return jnp.where(me == 0, first, everything[n:])

    def kernel(*refs):
        rows_refs, packed_ref = refs[:4], refs[4]
        part_refs, own_refs = refs[5 : 5 + n_parts], refs[5 + n_parts : 9 + n_parts]
        rows_out, factor, out_ref = refs[-3:]
        lane = lax.broadcasted_iota(jnp.int32, (1, LANES), 1)
        total = packed_ref[pl.ds(0, places.n_row), :]
        for part in part_refs:
            total = total + part[...]
        me = lax.axis_index("rep")
        mass = jnp.zeros((1, LANES), jnp.float32)
        out_ref[pl.ds(0, places.n_column), :] = packed_ref[pl.ds(places.n_row, places.n_column), :]
        out_ref[pl.ds(2 * places.n_column - 8, 8), :] = jnp.zeros((8, LANES), jnp.float32)
        news = []
        for k in range(4):
            at = slice(places.row_at[k], places.row_at[k] + places.blocks[k])
            r = moment_decay * old_rows(k, rows_refs[k], me) + (1.0 - moment_decay) / column_count[k] * total[at, :]
            news.append(r)
            mass = jnp.where(lane == k, jnp.sum(r), mass)
            rows_out[pl.ds(places.row_at[k], places.blocks[k]), :] = r
        fill = places.n_row - sum(places.blocks)
        if fill:
            rows_out[pl.ds(sum(places.blocks), fill), :] = jnp.ones((fill, LANES), jnp.float32)
        spread_rows(lax.rsqrt(jnp.concatenate(news, axis=0)), factor, sum(places.blocks))
        for k, m_ref in enumerate(own_refs):
            first = places.row_at[k] * LANES

            def step(i, sums):
                sums = list(sums)
                by_row = factor[pl.ds(pl.multiple_of(first + i * 8, 8), 8), :]
                for j in range(places.tiles[k]):
                    v = m_ref[pl.ds(pl.multiple_of(i * 8, 8), 8), pl.ds(j * LANES, LANES)] * by_row
                    sums[j] = sums[j] + v * v
                return tuple(sums)

            zero = jnp.zeros((8, LANES), jnp.float32)
            sums = lax.fori_loop(0, places.halves[k] // 8, step, (zero,) * places.tiles[k], unroll=2)
            for j in range(places.tiles[k]):
                at = pl.ds(places.n_column + places.column_at[k] + j, 1)
                out_ref[at, :] = jnp.sum(sums[j], axis=0, keepdims=True)
        out_ref[pl.ds(places.n_column + places.spare, 1), :] = mass

    return call(
        kernel,
        [*rows_old, packed, *row_parts, *own, *after],
        [struct(places.n_row, LANES), struct(sum(places.blocks) * LANES, LANES), struct(2 * places.n_column, LANES)],
        [VMEM] * (9 + n_parts) + [HBM] * len(after),
        [VMEM] * 3,
        cost=1 << 21,
    )


def columns(places, row_count, columns_old, total, other, after):
    def kernel(c0, c1, c2, c3, total_ref, other_ref, *rest):
        columns_out, out_ref = rest[-2:]
        old_refs = (c0, c1, c2, c3)
        lane = lax.broadcasted_iota(jnp.int32, (1, LANES), 1)
        both = total_ref[...] + other_ref[...]
        mass = jnp.zeros((1, LANES), jnp.float32)
        columns_out[pl.ds(places.n_column - 8, 8), :] = jnp.zeros((8, LANES), jnp.float32)
        row_mass = both[places.n_column + places.spare : places.n_column + places.spare + 1, :]
        for k in range(4):
            at = slice(places.column_at[k], places.column_at[k] + places.tiles[k])
            c = moment_decay * old_refs[k][...] + (1.0 - moment_decay) / row_count[k] * both[at, :]
            columns_out[pl.ds(places.column_at[k], places.tiles[k]), :] = c
            at = slice(places.n_column + at.start, places.n_column + at.stop)
            mass = jnp.where(lane == k, jnp.sum(both[at, :] / c), mass)
            mass = jnp.where(lane == 4 + k, jnp.sum(jnp.where(lane == k, row_mass, 0.0)), mass)
        out_ref[...] = jnp.broadcast_to(mass, (8, LANES))

    return call(
        kernel,
        [*columns_old, total, other, *after],
        [struct(places.n_column, LANES), struct(8, LANES)],
        [VMEM] * 6 + [HBM] * len(after),
        [VMEM] * 2,
        cost=1 << 20,
    )


def load_weights(weights, after):
    n = len(weights)

    def kernel(*refs):
        copies(list(zip(refs[:n], refs[n + 1 : 2 * n + 1])), refs[-1])

    return call(
        kernel,
        [*weights, after],
        [struct(*w.shape) for w in weights],
        [HBM] * n + [VMEM],
        [VMEM] * n,
        [pltpu.SemaphoreType.DMA((n,))],
        cost=1 << 24,
    )


def write_own(own, shapes, weights, after):
    n = len(weights)

    def kernel(*refs):
        me = lax.axis_index("rep")
        outs = refs[5 + n :]
        pairs = list(zip(refs[5 : 5 + n], outs[4 : 4 + n]))
        for k in range(4):
            h = refs[k].shape[0]
            pairs.append((refs[k], outs[k].at[pl.ds(pl.multiple_of(me * h, 8), h)]))
        copies(pairs, refs[-1])

    out = call(
        kernel,
        [*own, after, *weights],
        shapes + [struct(*w.shape) for w in weights],
        [VMEM] * 5 + [HBM] * n,
        [HBM] * 4 + [VMEM] * n,
        [pltpu.SemaphoreType.DMA((4 + n,))],
        cost=1 << 24,
    )
    return out[:4], out[4:]


def write_back(back, momenta):
    def kernel(*refs):
        me = lax.axis_index("rep")
        pairs = []
        for k in range(4):
            h = refs[k].shape[0]
            pairs.append((refs[k], refs[8 + k].at[pl.ds(pl.multiple_of((1 - me) * h, 8), h)]))
        copies(pairs, refs[-1])

    return call(
        kernel,
        [*back, *momenta],
        [struct(*m.shape) for m in momenta],
        [VMEM] * 4 + [HBM] * 4,
        [HBM] * 4,
        [pltpu.SemaphoreType.DMA((4,))],
        cost=1 << 24,
        aliases={4 + k: k for k in range(4)},
    )


def write_moments(places, rows_own, rows_other, columns_new):
    counts = [2 * h // LANES for h in places.halves]

    def kernel(own_ref, other_ref, columns_ref, *outs):
        me = lax.axis_index("rep")
        row_refs, column_refs = outs[:4], outs[4:8]
        spread_rows(lax.rsqrt(other_ref[...]), outs[8], sum(places.blocks))
        for k in range(4):
            h, n = places.halves[k], places.blocks[k]
            column_refs[k][...] = columns_ref[pl.ds(places.column_at[k], places.tiles[k]), :]
            mine = own_ref[pl.ds(places.row_at[k], n), :]
            other = other_ref[pl.ds(places.row_at[k], n), :]
            first = jnp.where(me == 0, mine, other)
            second = jnp.where(me == 0, other, mine)
            whole, rest = divmod(h, LANES)
            if not rest:
                row_refs[k][pl.ds(0, n), :] = first
                row_refs[k][pl.ds(n, n), :] = second
                continue
            turned = pltpu.roll(second, rest, 1)
            low = lax.broadcasted_iota(jnp.int32, (1, LANES), 1) < rest
            row_refs[k][pl.ds(0, whole), :] = first[:whole]
            before = first[whole : whole + 1]
            for i in range(counts[k] - whole):
                here = turned[i : i + 1]
                row_refs[k][pl.ds(whole + i, 1), :] = jnp.where(low, before, here)
                before = here

    ins = [pltpu.with_memory_space_constraint(x, pltpu.VMEM) for x in (rows_own, rows_other, columns_new)]
    out = pl.pallas_call(
        kernel,
        name="write_moments",
        out_shape=[struct(n, LANES) for n in counts + places.tiles]
        + [pltpu.VMEM((sum(places.blocks) * LANES, LANES), jnp.float32)],
        in_specs=[VMEM] * 3,
        out_specs=[VMEM] * 9,
        compiler_params=pltpu.CompilerParams(vmem_limit_bytes=2 << 20),
        cost_estimate=pl.CostEstimate(flops=1 << 24, bytes_accessed=0, transcendentals=0),
    )(*ins)
    return out[:4], out[4:8], out[8]


def write_weights(places, row_count, column_count, n_share, masses, factors, columns_new, own, back, weights, outs):
    n_parts = len(masses)

    def kernel(*refs):
        part_refs, refs = refs[:n_parts], refs[n_parts:]
        factor_refs, columns_ref = refs[:2], refs[2]
        own_refs, back_refs, w_refs, out_refs = (refs[3 + 4 * n : 7 + 4 * n] for n in range(4))
        stages, sem = refs[19:23], refs[23]
        me = lax.axis_index("rep")
        masses_all = sum((part[pl.ds(0, 1), :] for part in part_refs[1:]), part_refs[0][pl.ds(0, 1), :])
        lane = lax.broadcasted_iota(jnp.int32, (1, LANES), 1)

        def pick(n):
            return jnp.sum(jnp.where(lane == n, masses_all, 0.0), axis=1, keepdims=True)

        waits = []
        for k in range(4):
            h, tiles = places.halves[k], places.tiles[k]
            row_mean = pick(4 + k) / (n_share * row_count[k])
            spread = jnp.sqrt(pick(k) * row_mean / (row_count[k] * column_count[k]))
            scale = step_rate * jnp.sqrt(row_mean) / jnp.maximum(1.0, spread / clip_level)
            by_column = lax.rsqrt(columns_ref[pl.ds(places.column_at[k], tiles), :]) * scale
            wide = [jnp.broadcast_to(by_column[j : j + 1, :], (8, LANES)) for j in range(tiles)]
            chunk = h // PARTS if h % (8 * PARTS) == 0 else h
            first = places.row_at[k] * LANES
            for side, m_ref in enumerate((own_refs[k], back_refs[k])):
                which = me if side == 0 else 1 - me
                factor_ref = factor_refs[side]
                for begin in range(0, h, chunk):

                    def step(i, carry):
                        near = pl.multiple_of(begin + i * 8, 8)
                        far = pl.multiple_of(which * h + begin + i * 8, 8)
                        by_row = factor_ref[pl.ds(pl.multiple_of(first + begin + i * 8, 8), 8), :]
                        for j in range(tiles):
                            lanes = pl.ds(j * LANES, LANES)
                            change = m_ref[pl.ds(near, 8), lanes] * by_row * wide[j]
                            stages[k][pl.ds(far, 8), lanes] = w_refs[k][pl.ds(far, 8), lanes] - change
                        return carry

                    lax.fori_loop(0, chunk // 8, step, 0, unroll=2)
                    at = pl.ds(pl.multiple_of(which * h + begin, 8), chunk)
                    copy = pltpu.make_async_copy(stages[k].at[at], out_refs[k].at[at], sem.at[len(waits)])
                    copy.start()
                    waits.append(copy)
        for copy in waits:
            copy.wait()

    scratch = [pltpu.VMEM(w.shape, jnp.float32) for w in weights] + [pltpu.SemaphoreType.DMA((8 * PARTS,))]
    limit = sum(w.size * 4 for w in weights) + (4 << 20)
    return call(
        kernel,
        [*masses, *factors, columns_new, *own, *back, *weights],
        outs,
        [VMEM] * (n_parts + 15),
        [HBM] * 4,
        scratch,
        limit=limit,
        cost=1 << 22,
    )


def shifted(x, axis):
    n = lax.axis_size(axis)
    out = []
    for d in range(1, n):
        if n & (n - 1):
            pairs = [(i, (i + d) % n) for i in range(n)]
        else:
            pairs = [(i, i ^ d) for i in range(n)]
        out.append(lax.ppermute(x, axis, pairs))
    return out


def fast_body(*args):
    weights, momenta, partials, rows, columns_in = (args[k::5] for k in range(5))
    n_fs, n_tp = lax.axis_size("fs"), lax.axis_size("tp")
    heights = [item.shape[0] for item in weights]
    widths = [item.shape[1] for item in weights]
    row_count = [h * n_fs for h in heights]
    column_count = [w * n_tp for w in widths]
    places = Places(heights, widths)
    shapes = [struct(*w.shape) for w in weights]

    received = [None] * 4
    for group in (ORDER[:1], ORDER[1:]):
        for k, other in zip(group, other_halves([partials[k] for k in group])):
            received[k] = swap(other)
    halves = own_halves([*partials, *momenta])
    rows_old = [item.reshape(-1, LANES) for item in rows]
    columns_old = [item.reshape(-1, LANES) for item in columns_in]
    own, back, packed = [None] * 4, [None] * 4, None
    for k in ORDER:
        own[k], packed = statistics(k, places, halves[k], halves[4 + k], received[k], packed)
        back[k] = swap(own[k])

    row_parts = shifted(packed[: places.n_row], "tp")
    held_first = load_weights([weights[0], weights[3]], packed)
    rows_own, factor_own, local = shares(places, column_count, rows_old, row_parts, packed, own, ())

    rows_other = swap(rows_own)
    total = sum(shifted(local, "fs"), local)
    momenta_next, held_second = write_own(own, shapes, [weights[1], weights[2]], local)
    momenta_next = write_back(back, momenta_next)
    columns_new, mass = columns(places, row_count, columns_old, total, swap(total), ())

    held = [held_first[0], *held_second, held_first[1]]
    masses = [mass, *shifted(mass, "tp")]
    rows_new, columns_out, factor_other = write_moments(places, rows_own, rows_other, columns_new)
    weights_next = write_weights(
        places, row_count, column_count, n_tp, masses, [factor_own, factor_other], columns_new, own, back, held, shapes
    )
    out = []
    for k in range(4):
        out += [weights_next[k], momenta_next[k], rows_new[k].reshape(-1), columns_out[k].reshape(-1)]
    return tuple(out)


def half(x, which):
    size = x.shape[0] // 2
    return lax.dynamic_slice_in_dim(x, which * size, size, 0)


def join(own, other, me):
    first = me == 0
    return jnp.concatenate([jnp.where(first, own, other), jnp.where(first, other, own)], axis=0)


def cross_sums(row_part, column_part, me):
    n_fs, n_tp = lax.axis_size("fs"), lax.axis_size("tp")
    if n_fs != n_tp:
        return lax.psum(row_part, "tp"), lax.psum(column_part, "fs")
    length = max(row_part.size, column_part.size)

    def padded(x):
        return jnp.pad(x, (0, length - x.size))

    mine = jnp.where(me == 1, padded(row_part), padded(column_part))
    total = mine
    for shift in range(1, n_tp):
        pairs = []
        for f in range(n_fs):
            for t in range(n_tp):
                here = (f * n_tp + t) * 2
                pairs.append((here + 1, (f * n_tp + (t + shift) % n_tp) * 2 + 1))
                pairs.append((here, ((f + shift) % n_fs * n_tp + t) * 2))
        total = total + lax.ppermute(mine, EVERY, pairs)
    other = swap(total)
    rows = jnp.where(me == 1, total, other)[: row_part.size]
    columns = jnp.where(me == 1, other, total)[: column_part.size]
    return rows, columns


def plain_body(*args):
    weights, momenta, partials, rows, columns = (args[k::5] for k in range(5))
    me = lax.axis_index("rep")
    n_all = lax.axis_size(EVERY)
    partials = [item[0] for item in partials]
    heights = [item.shape[0] for item in weights]
    widths = [item.shape[1] for item in weights]
    row_count = [h * lax.axis_size("fs") for h in heights]
    column_count = [w * lax.axis_size("tp") for w in widths]

    received = [None] * 4
    for k in ORDER:
        received[k] = swap(half(partials[k], 1 - me))
    own = [None] * 4
    back = [None] * 4
    row_local = [None] * 4
    column_local = [None] * 4
    for k in ORDER:
        grad = half(partials[k], me) + received[k]
        own[k] = momentum_decay * half(momenta[k], me) + (1.0 - momentum_decay) * grad
        back[k] = swap(own[k])
        square = grad * grad
        placed = jnp.zeros((heights[k],), jnp.float32)
        row_local[k] = lax.dynamic_update_slice_in_dim(
            placed, jnp.sum(square, axis=1), me * (heights[k] // 2), 0
        )
        column_local[k] = jnp.sum(square, axis=0)

    local = jnp.concatenate(row_local + column_local)
    local = local + swap(local)
    n_rows = sum(heights)
    row_total, column_total = cross_sums(local[:n_rows], local[n_rows:], me)

    rows_next, columns_next = [], []
    at_row = at_column = 0
    for k in range(4):
        r = row_total[at_row : at_row + heights[k]]
        c = column_total[at_column : at_column + widths[k]]
        at_row += heights[k]
        at_column += widths[k]
        rows_next.append(moment_decay * rows[k] + (1.0 - moment_decay) * r / column_count[k])
        columns_next.append(moment_decay * columns[k] + (1.0 - moment_decay) * c / row_count[k])

    mass = []
    for k in range(4):
        m = own[k]
        mass.append(jnp.sum(m * m / half(rows_next[k], me)[:, None] / columns_next[k][None, :]))
    row_mass = [jnp.sum(half(rows_next[k], me)) for k in range(4)]
    scalars = jnp.stack(mass + row_mass)
    spread_out = jnp.broadcast_to(scalars[None], (n_all, 8))
    totals = jnp.sum(lax.all_to_all(spread_out, EVERY, 0, 0), axis=0)

    weights_next, momenta_next = [], []
    for k in range(4):
        row_mean = totals[4 + k] / (lax.axis_size("tp") * row_count[k])
        spread = jnp.sqrt(totals[k] * row_mean / (row_count[k] * column_count[k]))
        factor = jnp.maximum(1.0, spread / clip_level)
        scale = step_rate * jnp.sqrt(row_mean) / factor
        m = join(own[k], back[k], me)
        momenta_next.append(m)
        by_row = lax.rsqrt(rows_next[k]) * scale
        by_column = lax.rsqrt(columns_next[k])
        weights_next.append(weights[k] - m * by_row[:, None] * by_column[None, :])
    out = []
    for k in range(4):
        out += [weights_next[k], momenta_next[k], rows_next[k], columns_next[k]]
    return tuple(out)


def fits(args):
    small = max(lax.axis_size("fs"), lax.axis_size("tp")) <= 8
    return small and all(n % LANES == 0 for item in args[0::5] for n in item.shape)


def body(*args):
    return fast_body(*args) if fits(args) else plain_body(*args)


def solution(mesh):
    matrix, stacked = P("fs", "tp"), P("rep", "fs", "tp")

    return jax.shard_map(
        body,
        mesh=mesh,
        in_specs=(matrix, matrix, stacked, P("fs"), P("tp")) * 4,
        out_specs=(matrix, matrix, P("fs"), P("tp")) * 4,
        check_vma=False,
    )
```

profile of v0, /device:TPU:0, one launch (start us, length us, event | category | flops | bytes accessed | tf_op | source)
XLA Modules:
  0.0 67.9 jit_solution(3001564669695097321)
XLA Ops:
  0.6 1.4 %shard_map.317 = f32[256,1408]{1,0:T(8,128)S(1)} custom-call(f32[1,512,1408]{2,1,0:T(8,128)} %refs_0_.6), custom_call_target="tpu_custom_call" | custom-call | flops 2097152 | tf_op jit(solution)/shard_map/pallas_call | solution.py:34
  2.0 0.6 collective-permute-start.3
  2.6 1.9 %shard_map.316 = (f32[256,1408]{1,0:T(8,128)S(1)}, f32[704,512]{1,0:T(8,128)S(1)}, f32[256,512]{1,0:T(8,128)S(1)}) custom-call(f32[1,512,1408]{2,1,0:T(8,128)} %refs_0_.5, f32[1,1408,512]{2,1,0:T(8,128)} %refs_1_.4, f32[1,512,512]{2,1,0:T(8,128)} %refs_2_.3), custom_call_target="tpu_custom_call" | custom-call | flops 2097152 | tf_op jit(solution)/shard_map/pallas_call | solution.py:34
  4.5 0.1 collective-permute-start.2
  4.6 0.5 collective-permute-start.1
  5.1 3.8 %shard_map.315 = (f32[256,1408]{1,0:T(8,128)S(1)}, f32[256,1408]{1,0:T(8,128)S(1)}, f32[704,512]{1,0:T(8,128)S(1)}, f32[256,512]{1,0:T(8,128)S(1)}, f32[256,1408...) custom-call(f32[1,512,1408]{2,1,0:T(8,128)} %refs_0_.6, ...), custom_call_target="tpu_custom_call" | custom-call | flops 4194304 | tf_op jit(solution)/shard_map/pallas_call | solution.py:34
  8.9 0.0 collective-permute-done.3.refs_2_
  9.0 0.6 shard_map.318
  9.6 0.0 collective-permute-done.2.refs_2_
  9.6 0.6 shard_map.319
  10.2 0.0 collective-permute-done.1.refs_2_
  10.2 0.0 copy-start
  10.2 0.0 copy-start.3
  10.2 0.0 copy-start.4
  10.2 0.0 copy-start.5
  10.2 0.8 %shard_map.320 = (f32[704,512]{1,0:T(8,128)S(1)}, f32[48,128]{1,0:T(8,128)S(1)}) custom-call(f32[704,512]{1,0:T(8,128)S(1)} %get-tuple-element.68.refs_0_, f32[704,512]{1,0:T(8,128)S(1)} %get-tuple-element.69.refs_1_, f32[704,512]{1,0:T(8,128)S(1)} %collective-permute-done.1.refs_2_, ...), custom_call_target="tpu_custom_call", output_to_operand_aliasing={{1}: (3, {})} | custom-call | flops 1048576 | tf_op jit(solution)/shard_map/pallas_call | solution.py:34
  11.0 0.2 collective-permute-start.17
  11.2 0.4 collective-permute-start.16
  11.6 0.1 collective-permute-start.15
  11.7 0.4 collective-permute-start
  12.1 7.1 %collective-permute-done.refs_2_ = f32[256,512]{1,0:T(8,128)S(1)} collective-permute-done((f32[256,512]{1,0:T(8,128)S(1)}, f32[256,512]{1,0:T(8,128)S(1)}, u32[]{:S(2)}, u32[]{:S(2)}) %collective-permute-start) | collective-permute-done | bytes 524320 | tf_op jit(solution)/shard_map/ppermute | solution.py:47
  19.2 0.3 shard_map.321
  19.5 0.2 collective-permute-start.18
  19.7 3.8 %collective-permute-start.6 = (f32[16,128]{1,0:T(8,128)S(1)}, f32[16,128]{1,0:T(8,128)S(1)}, u32[]{:S(2)}, u32[]{:S(2)}) collective-permute-start(f32[16,128]{1,0:T(8,128)S(1)} %slice.3), channel_id=1, source_target_pairs={{0,6},{2,4},{4,2},{6,0},{1,7},{3,5},{5,3},{7,1},{8,14},{10,12},{12... | collective-permute-start | bytes 24584 | tf_op jit(solution)/shard_map/ppermute | solution.py:430
  23.6 1.6 %collective-permute-done.6.refs_7_ = f32[16,128]{1,0:T(8,128)S(1)} collective-permute-done((f32[16,128]{1,0:T(8,128)S(1)}, f32[16,128]{1,0:T(8,128)S(1)}, u32[]{:S(2)}, u32[]{:S(2)}) %collective-permute-start.6) | collective-permute-done | bytes 8224 | tf_op jit(solution)/shard_map/ppermute | solution.py:430
  25.2 2.0 %collective-permute-start.5 = (f32[16,128]{1,0:T(8,128)S(1)}, f32[16,128]{1,0:T(8,128)S(1)}, u32[]{:S(2)}, u32[]{:S(2)}) collective-permute-start(f32[16,128]{1,0:T(8,128)S(1)} %slice.3), channel_id=1, source_target_pairs={{0,4},{2,6},{4,0},{6,2},{1,5},{3,7},{5,1},{7,3},{8,12},{10,14},{12... | collective-permute-start | bytes 24584 | tf_op jit(solution)/shard_map/ppermute | solution.py:430
  27.2 1.7 %collective-permute-done.5.refs_6_ = f32[16,128]{1,0:T(8,128)S(1)} collective-permute-done((f32[16,128]{1,0:T(8,128)S(1)}, f32[16,128]{1,0:T(8,128)S(1)}, u32[]{:S(2)}, u32[]{:S(2)}) %collective-permute-start.5) | collective-permute-done | bytes 8224 | tf_op jit(solution)/shard_map/ppermute | solution.py:430
  28.8 2.0 %collective-permute-start.4 = (f32[16,128]{1,0:T(8,128)S(1)}, f32[16,128]{1,0:T(8,128)S(1)}, u32[]{:S(2)}, u32[]{:S(2)}) collective-permute-start(f32[16,128]{1,0:T(8,128)S(1)} %slice.3), channel_id=1, source_target_pairs={{0,2},{2,0},{4,6},{6,4},{1,3},{3,1},{5,7},{7,5},{8,10},{10,8},{12,... | collective-permute-start | bytes 24584 | tf_op jit(solution)/shard_map/ppermute | solution.py:430
  30.8 1.7 %collective-permute-done.4.refs_5_ = f32[16,128]{1,0:T(8,128)S(1)} collective-permute-done((f32[16,128]{1,0:T(8,128)S(1)}, f32[16,128]{1,0:T(8,128)S(1)}, u32[]{:S(2)}, u32[]{:S(2)}) %collective-permute-start.4) | collective-permute-done | bytes 8224 | tf_op jit(solution)/shard_map/ppermute | solution.py:430
  32.5 0.0 copy-done
  32.5 0.0 copy-done.3
  32.5 0.0 copy-done.4
  32.5 0.0 copy-done.5
  32.5 1.4 %shard_map.322 = (f32[16,128]{1,0:T(8,128)S(1)}, f32[1536,128]{1,0:T(8,128)S(1)}, f32[64,128]{1,0:T(8,128)S(1)}) custom-call(f32[4,128]{1,0:T(4,128)S(1)} %bitcast.19, f32[4,128]{1,0:T(4,128)S(1)} %bitcast.20, f32[11,128]{1,0:T(8,128)S(1)} %bitcast.16, f32[4,128]{1,0:T(4,128)S(1)} %bitcast.21, f32[48,128]{1,0:T(8,128)S(1)} %get-tuple-element.79.refs_4_.refs_2_, ...), custom_call_target="tpu_custom_call" | custom-call | flops 2097152 | tf_op jit(solution)/shard_map/pallas_call | solution.py:34
  33.9 0.0 copy-start.1
  33.9 0.0 copy-start.2
  33.9 0.0 copy-start.6
  33.9 0.0 copy-start.7
  34.0 4.1 %collective-permute-start.9 = (f32[64,128]{1,0:T(8,128)S(1)}, f32[64,128]{1,0:T(8,128)S(1)}, u32[]{:S(2)}, u32[]{:S(2)}) collective-permute-start(f32[64,128]{1,0:T(8,128)S(1)} %get-tuple-element.84.refs_4_), channel_id=1, source_target_pairs={{0,24},{8,16},{16,8},{24,0},{1,25},{9,17},{17,9},{25,1},{2,26},{10... | collective-permute-start | bytes 98312 | tf_op jit(solution)/shard_map/ppermute | solution.py:430
  38.1 2.0 %collective-permute-done.9 = f32[64,128]{1,0:T(8,128)S(1)} collective-permute-done((f32[64,128]{1,0:T(8,128)S(1)}, f32[64,128]{1,0:T(8,128)S(1)}, u32[]{:S(2)}, u32[]{:S(2)}) %collective-permute-start.9) | collective-permute-done | bytes 32800 | tf_op jit(solution)/shard_map/ppermute | solution.py:430
  40.1 0.9 %collective-permute-start.8 = (f32[64,128]{1,0:T(8,128)S(1)}, f32[64,128]{1,0:T(8,128)S(1)}, u32[]{:S(2)}, u32[]{:S(2)}) collective-permute-start(f32[64,128]{1,0:T(8,128)S(1)} %get-tuple-element.84.refs_4_), channel_id=1, source_target_pairs={{0,16},{8,24},{16,0},{24,8},{1,17},{9,25},{17,1},{25,9},{2,18},{10... | collective-permute-start | bytes 98312 | tf_op jit(solution)/shard_map/ppermute | solution.py:430
  41.0 3.9 %collective-permute-done.8 = f32[64,128]{1,0:T(8,128)S(1)} collective-permute-done((f32[64,128]{1,0:T(8,128)S(1)}, f32[64,128]{1,0:T(8,128)S(1)}, u32[]{:S(2)}, u32[]{:S(2)}) %collective-permute-start.8) | collective-permute-done | bytes 32800 | tf_op jit(solution)/shard_map/ppermute | solution.py:430
  44.9 1.4 %collective-permute-start.7 = (f32[64,128]{1,0:T(8,128)S(1)}, f32[64,128]{1,0:T(8,128)S(1)}, u32[]{:S(2)}, u32[]{:S(2)}) collective-permute-start(f32[64,128]{1,0:T(8,128)S(1)} %get-tuple-element.84.refs_4_), channel_id=1, source_target_pairs={{0,8},{8,0},{16,24},{24,16},{1,9},{9,1},{17,25},{25,17},{2,10},{10... | collective-permute-start | bytes 98312 | tf_op jit(solution)/shard_map/ppermute | solution.py:430
  46.3 2.6 %collective-permute-done.7 = f32[64,128]{1,0:T(8,128)S(1)} collective-permute-done((f32[64,128]{1,0:T(8,128)S(1)}, f32[64,128]{1,0:T(8,128)S(1)}, u32[]{:S(2)}, u32[]{:S(2)}) %collective-permute-start.7) | collective-permute-done | bytes 32800 | tf_op jit(solution)/shard_map/ppermute | solution.py:430
  48.8 0.1 collective-permute-start.10
  48.9 1.2 %collective-permute-done.10.other_ref = f32[64,128]{1,0:T(8,128)S(1)} collective-permute-done((f32[64,128]{1,0:T(8,128)S(1)}, f32[64,128]{1,0:T(8,128)S(1)}, u32[]{:S(2)}, u32[]{:S(2)}) %collective-permute-start.10) | collective-permute-done | bytes 32800 | tf_op jit(solution)/shard_map/ppermute | solution.py:47
  50.1 0.2 collective-permute-start.14
  50.3 2.1 %shard_map.324 = (f32[512,1408]{1,0:T(8,128)S(1)}, f32[512,512]{1,0:T(8,128)S(1)}) custom-call(f32[512,1408]{1,0:T(8,128)} %refs_0_.7, f32[512,512]{1,0:T(8,128)} %refs_1_.5, f32[48,128]{1,0:T(8,128)S(1)} %get-tuple-element.79.refs_4_.refs_2_), custom_call_target="tpu_custom_call" | custom-call | flops 16777216 | tf_op jit(solution)/shard_map/pallas_call | solution.py:34
  52.4 0.1 shard_map.323
  52.6 0.0 collective-permute-done.14.other_ref
  52.6 2.6 %collective-permute-start.13 = (f32[8,128]{1,0:T(8,128)S(1)}, f32[8,128]{1,0:T(8,128)S(1)}, u32[]{:S(2)}, u32[]{:S(2)}) collective-permute-start(f32[8,128]{1,0:T(8,128)S(1)} %get-tuple-element.85.refs_0_), channel_id=1, source_target_pairs={{0,6},{2,4},{4,2},{6,0},{1,7},{3,5},{5,3},{7,1},{8,14},{10,12},{12... | collective-permute-start | bytes 12296 | tf_op jit(solution)/shard_map/ppermute | solution.py:430
  55.2 0.0 collective-permute-done.18.refs_14_.refs_3_
  55.2 0.5 collective-permute-start.12
  55.7 0.0 collective-permute-done.17.refs_13_.refs_2_
  55.7 0.4 collective-permute-start.11
  56.2 4.5 %shard_map.325 = (f32[512,1408]{1,0:T(8,128)}, f32[512,1408]{1,0:T(8,128)}, f32[1408,512]{1,0:T(8,128)}, f32[512,512]{1,0:T(8,128)}, f32[512,1408]{1,0:T(8,128)S(1)}, /*index=5*/f32[1408,512]{1,0:T(8,128)S(1)}) custom-call(f32[256,1408]{1,0:T(8,128)S(1)} %get-tuple-element.80.refs_8_.refs_0_.refs_7_, ...), custom_call_target="tpu_custom_call" | custom-call | flops 16777216 | tf_op jit(solution)/shard_map/pallas_call | solution.py:34
  60.6 0.8 %write_moments.1 = (f32[4,128]{1,0:T(4,128)}, f32[4,128]{1,0:T(4,128)}, f32[11,128]{1,0:T(8,128)}, f32[4,128]{1,0:T(4,128)}, f32[11,128]{1,0:T(8,128)}, /*index=...) custom-call(f32[16,128]{1,0:T(8,128)S(1)} %get-tuple-element.87.own_ref, ...), custom_call_target="tpu_custom_call" | custom-call | flops 16777216 | tf_op jit(solution)/shard_map/write_moments/pallas_call | solution.py:347
  61.5 0.0 collective-permute-done.16.refs_12_.refs_1_
  61.5 0.0 collective-permute-done.15.refs_11_.refs_0_
  61.5 2.3 %shard_map.327 = (f32[512,1408]{1,0:T(8,128)}, f32[512,1408]{1,0:T(8,128)}, f32[1408,512]{1,0:T(8,128)}, f32[512,512]{1,0:T(8,128)}) custom-call(f32[256,1408]{1,0:T(8,128)S(1)} %collective-permute-done.15.refs_11_.refs_0_, ...), custom_call_target="tpu_custom_call", output_to_operand_aliasing={{0}: (4, {}), {1}: (5, {}), {2}: (6, {}), {3}: (7, {})} | custom-call | flops 16777216 | tf_op jit(solution)/shard_map/pallas_call | solution.py:34
  63.8 0.0 collective-permute-done.13.refs_3_
  63.8 0.0 collective-permute-done.12.refs_2_
  63.8 0.0 collective-permute-done.11.refs_1_
  63.8 4.1 %shard_map.326 = (f32[512,1408]{1,0:T(8,128)}, f32[512,1408]{1,0:T(8,128)}, f32[1408,512]{1,0:T(8,128)}, f32[512,512]{1,0:T(8,128)}) custom-call(f32[8,128]{1,0:T(8,128)S(1)} %get-tuple-element.85.refs_0_, f32[8,128]{1,0:T(8,128)S(1)} %collective-permute-done.11.refs_1_, f32[8,128]{1,0:T(8,128)S(1)} %collective-permute-done.12.refs_2_, ...), custom_call_target="tpu_custom_call" | custom-call | flops 4194304 | tf_op jit(solution)/shard_map/pallas_call | solution.py:34
  (6 shorter events, 0.0 us)
Async XLA Ops:
  2.0 6.9 %collective-permute-start.3 = (f32[256,1408]{1,0:T(8,128)S(1)}, f32[256,1408]{1,0:T(8,128)S(1)}, u32[]{:S(2)}, u32[]{:S(2)}) collective-permute-start(f32[256,1408]{1,0:T(8,128)S(1)} %shard_map.317), channel_id=1, source_target_pairs={{0,1},{1,0},{2,3},{3,2},{4,5},{5,4},{6,7},{7,6},{8,9},{9,8},{10,11... | collective-permute-start | bytes 4325384 | tf_op jit(solution)/shard_map/ppermute | solution.py:47
  4.5 5.0 %collective-permute-start.2 = (f32[256,1408]{1,0:T(8,128)S(1)}, f32[256,1408]{1,0:T(8,128)S(1)}, u32[]{:S(2)}, u32[]{:S(2)}) collective-permute-start(f32[256,1408]{1,0:T(8,128)S(1)} %get-tuple-element.73), channel_id=1, source_target_pairs={{0,1},{1,0},{2,3},{3,2},{4,5},{5,4},{6,7},{7,6},{8,9},{9,8},{10,11... | collective-permute-start | bytes 4325384 | tf_op jit(solution)/shard_map/ppermute | solution.py:47
  4.6 5.6 %collective-permute-start.1 = (f32[704,512]{1,0:T(8,128)S(1)}, f32[704,512]{1,0:T(8,128)S(1)}, u32[]{:S(2)}, u32[]{:S(2)}) collective-permute-start(f32[704,512]{1,0:T(8,128)S(1)} %get-tuple-element.70), channel_id=1, source_target_pairs={{0,1},{1,0},{2,3},{3,2},{4,5},{5,4},{6,7},{7,6},{8,9},{9,8},{10,11... | collective-permute-start | bytes 4325384 | tf_op jit(solution)/shard_map/ppermute | solution.py:47
  10.2 22.3 %copy-start = (f32[1408]{0:T(1024)S(1)}, f32[1408]{0:T(1024)}, u32[]{:S(2)}) copy-start(f32[1408]{0:T(1024)} %param.33) | copy-start | bytes 16900
  10.2 22.3 %copy-start.3 = (f32[512]{0:T(512)S(1)}, f32[512]{0:T(512)}, u32[]{:S(2)}) copy-start(f32[512]{0:T(512)} %param.23) | copy-start | bytes 6148
  10.2 22.3 %copy-start.4 = (f32[512]{0:T(512)S(1)}, f32[512]{0:T(512)}, u32[]{:S(2)}) copy-start(f32[512]{0:T(512)} %param.28) | copy-start | bytes 6148
  10.2 22.3 %copy-start.5 = (f32[512]{0:T(512)S(1)}, f32[512]{0:T(512)}, u32[]{:S(2)}) copy-start(f32[512]{0:T(512)} %param.38) | copy-start | bytes 6148
  11.0 44.7 %collective-permute-start.17 = (f32[704,512]{1,0:T(8,128)S(1)}, f32[704,512]{1,0:T(8,128)S(1)}, u32[]{:S(2)}, u32[]{:S(2)}) collective-permute-start(f32[704,512]{1,0:T(8,128)S(1)} %get-tuple-element.82.refs_10_.refs_2_.refs_9_), channel_id=1, source_target_pairs={{0,1},{1,0},{2,3},{3,2},{4,5},{5,4},{6,7},{7,6},{8,9},{9,8},{10,11... | collective-permute-start | bytes 4325384 | tf_op jit(solution)/shard_map/ppermute | solution.py:47
  11.2 50.3 %collective-permute-start.16 = (f32[256,1408]{1,0:T(8,128)S(1)}, f32[256,1408]{1,0:T(8,128)S(1)}, u32[]{:S(2)}, u32[]{:S(2)}) collective-permute-start(f32[256,1408]{1,0:T(8,128)S(1)} %get-tuple-element.81.refs_9_.refs_1_.refs_8_), channel_id=1, source_target_pairs={{0,1},{1,0},{2,3},{3,2},{4,5},{5,4},{6,7},{7,6},{8,9},{9,8},{10,11... | collective-permute-start | bytes 4325384 | tf_op jit(solution)/shard_map/ppermute | solution.py:47
  11.6 49.9 %collective-permute-start.15 = (f32[256,1408]{1,0:T(8,128)S(1)}, f32[256,1408]{1,0:T(8,128)S(1)}, u32[]{:S(2)}, u32[]{:S(2)}) collective-permute-start(f32[256,1408]{1,0:T(8,128)S(1)} %get-tuple-element.80.refs_8_.refs_0_.refs_7_), channel_id=1, source_target_pairs={{0,1},{1,0},{2,3},{3,2},{4,5},{5,4},{6,7},{7,6},{8,9},{9,8},{10,11... | collective-permute-start | bytes 4325384 | tf_op jit(solution)/shard_map/ppermute | solution.py:47
  11.7 7.5 %collective-permute-start = (f32[256,512]{1,0:T(8,128)S(1)}, f32[256,512]{1,0:T(8,128)S(1)}, u32[]{:S(2)}, u32[]{:S(2)}) collective-permute-start(f32[256,512]{1,0:T(8,128)S(1)} %get-tuple-element.67), channel_id=1, source_target_pairs={{0,1},{1,0},{2,3},{3,2},{4,5},{5,4},{6,7},{7,6},{8,9},{9,8},{10,11... | collective-permute-start | bytes 1572872 | tf_op jit(solution)/shard_map/ppermute | solution.py:47
  19.5 35.7 %collective-permute-start.18 = (f32[256,512]{1,0:T(8,128)S(1)}, f32[256,512]{1,0:T(8,128)S(1)}, u32[]{:S(2)}, u32[]{:S(2)}) collective-permute-start(f32[256,512]{1,0:T(8,128)S(1)} %get-tuple-element.83.refs_11_.refs_3_.refs_10_), channel_id=1, source_target_pairs={{0,1},{1,0},{2,3},{3,2},{4,5},{5,4},{6,7},{7,6},{8,9},{9,8},{10,11... | collective-permute-start | bytes 1572872 | tf_op jit(solution)/shard_map/ppermute | solution.py:47
  19.7 5.5 %collective-permute-start.6 = (f32[16,128]{1,0:T(8,128)S(1)}, f32[16,128]{1,0:T(8,128)S(1)}, u32[]{:S(2)}, u32[]{:S(2)}) collective-permute-start(f32[16,128]{1,0:T(8,128)S(1)} %slice.3), channel_id=1, source_target_pairs={{0,6},{2,4},{4,2},{6,0},{1,7},{3,5},{5,3},{7,1},{8,14},{10,12},{12... | collective-permute-start | bytes 24584 | tf_op jit(solution)/shard_map/ppermute | solution.py:430
  25.2 3.7 %collective-permute-start.5 = (f32[16,128]{1,0:T(8,128)S(1)}, f32[16,128]{1,0:T(8,128)S(1)}, u32[]{:S(2)}, u32[]{:S(2)}) collective-permute-start(f32[16,128]{1,0:T(8,128)S(1)} %slice.3), channel_id=1, source_target_pairs={{0,4},{2,6},{4,0},{6,2},{1,5},{3,7},{5,1},{7,3},{8,12},{10,14},{12... | collective-permute-start | bytes 24584 | tf_op jit(solution)/shard_map/ppermute | solution.py:430
  28.8 3.7 %collective-permute-start.4 = (f32[16,128]{1,0:T(8,128)S(1)}, f32[16,128]{1,0:T(8,128)S(1)}, u32[]{:S(2)}, u32[]{:S(2)}) collective-permute-start(f32[16,128]{1,0:T(8,128)S(1)} %slice.3), channel_id=1, source_target_pairs={{0,2},{2,0},{4,6},{6,4},{1,3},{3,1},{5,7},{7,5},{8,10},{10,8},{12,... | collective-permute-start | bytes 24584 | tf_op jit(solution)/shard_map/ppermute | solution.py:430
  33.9 18.5 %copy-start.1 = (f32[1408]{0:T(1024)S(1)}, f32[1408]{0:T(1024)}, u32[]{:S(2)}) copy-start(f32[1408]{0:T(1024)} %param.24) | copy-start | bytes 16900
  33.9 18.5 %copy-start.2 = (f32[1408]{0:T(1024)S(1)}, f32[1408]{0:T(1024)}, u32[]{:S(2)}) copy-start(f32[1408]{0:T(1024)} %param.29) | copy-start | bytes 16900
  33.9 18.5 %copy-start.6 = (f32[512]{0:T(512)S(1)}, f32[512]{0:T(512)}, u32[]{:S(2)}) copy-start(f32[512]{0:T(512)} %param.34) | copy-start | bytes 6148
  33.9 18.5 %copy-start.7 = (f32[512]{0:T(512)S(1)}, f32[512]{0:T(512)}, u32[]{:S(2)}) copy-start(f32[512]{0:T(512)} %param.39) | copy-start | bytes 6148
  34.0 6.1 %collective-permute-start.9 = (f32[64,128]{1,0:T(8,128)S(1)}, f32[64,128]{1,0:T(8,128)S(1)}, u32[]{:S(2)}, u32[]{:S(2)}) collective-permute-start(f32[64,128]{1,0:T(8,128)S(1)} %get-tuple-element.84.refs_4_), channel_id=1, source_target_pairs={{0,24},{8,16},{16,8},{24,0},{1,25},{9,17},{17,9},{25,1},{2,26},{10... | collective-permute-start | bytes 98312 | tf_op jit(solution)/shard_map/ppermute | solution.py:430
  40.1 4.8 %collective-permute-start.8 = (f32[64,128]{1,0:T(8,128)S(1)}, f32[64,128]{1,0:T(8,128)S(1)}, u32[]{:S(2)}, u32[]{:S(2)}) collective-permute-start(f32[64,128]{1,0:T(8,128)S(1)} %get-tuple-element.84.refs_4_), channel_id=1, source_target_pairs={{0,16},{8,24},{16,0},{24,8},{1,17},{9,25},{17,1},{25,9},{2,18},{10... | collective-permute-start | bytes 98312 | tf_op jit(solution)/shard_map/ppermute | solution.py:430
  44.9 3.9 %collective-permute-start.7 = (f32[64,128]{1,0:T(8,128)S(1)}, f32[64,128]{1,0:T(8,128)S(1)}, u32[]{:S(2)}, u32[]{:S(2)}) collective-permute-start(f32[64,128]{1,0:T(8,128)S(1)} %get-tuple-element.84.refs_4_), channel_id=1, source_target_pairs={{0,8},{8,0},{16,24},{24,16},{1,9},{9,1},{17,25},{25,17},{2,10},{10... | collective-permute-start | bytes 98312 | tf_op jit(solution)/shard_map/ppermute | solution.py:430
  48.8 1.3 %collective-permute-start.10 = (f32[64,128]{1,0:T(8,128)S(1)}, f32[64,128]{1,0:T(8,128)S(1)}, u32[]{:S(2)}, u32[]{:S(2)}) collective-permute-start(f32[64,128]{1,0:T(8,128)S(1)} %add_add_fusion.total_ref), channel_id=1, source_target_pairs={{0,1},{1,0},{2,3},{3,2},{4,5},{5,4},{6,7},{7,6},{8,9},{9,8},{10,11... | collective-permute-start | bytes 98312 | tf_op jit(solution)/shard_map/ppermute | solution.py:47
  50.1 2.5 %collective-permute-start.14 = (f32[16,128]{1,0:T(8,128)S(1)}, f32[16,128]{1,0:T(8,128)S(1)}, u32[]{:S(2)}, u32[]{:S(2)}) collective-permute-start(f32[16,128]{1,0:T(8,128)S(1)} %get-tuple-element.87.own_ref), channel_id=1, source_target_pairs={{0,1},{1,0},{2,3},{3,2},{4,5},{5,4},{6,7},{7,6},{8,9},{9,8},{10,11... | collective-permute-start | bytes 24584 | tf_op jit(solution)/shard_map/ppermute | solution.py:47
  52.6 11.2 %collective-permute-start.13 = (f32[8,128]{1,0:T(8,128)S(1)}, f32[8,128]{1,0:T(8,128)S(1)}, u32[]{:S(2)}, u32[]{:S(2)}) collective-permute-start(f32[8,128]{1,0:T(8,128)S(1)} %get-tuple-element.85.refs_0_), channel_id=1, source_target_pairs={{0,6},{2,4},{4,2},{6,0},{1,7},{3,5},{5,3},{7,1},{8,14},{10,12},{12... | collective-permute-start | bytes 12296 | tf_op jit(solution)/shard_map/ppermute | solution.py:430
  55.2 8.5 %collective-permute-start.12 = (f32[8,128]{1,0:T(8,128)S(1)}, f32[8,128]{1,0:T(8,128)S(1)}, u32[]{:S(2)}, u32[]{:S(2)}) collective-permute-start(f32[8,128]{1,0:T(8,128)S(1)} %get-tuple-element.85.refs_0_), channel_id=1, source_target_pairs={{0,4},{2,6},{4,0},{6,2},{1,5},{3,7},{5,1},{7,3},{8,12},{10,14},{12... | collective-permute-start | bytes 12296 | tf_op jit(solution)/shard_map/ppermute | solution.py:430
  55.7 8.0 %collective-permute-start.11 = (f32[8,128]{1,0:T(8,128)S(1)}, f32[8,128]{1,0:T(8,128)S(1)}, u32[]{:S(2)}, u32[]{:S(2)}) collective-permute-start(f32[8,128]{1,0:T(8,128)S(1)} %get-tuple-element.85.refs_0_), channel_id=1, source_target_pairs={{0,2},{2,0},{4,6},{6,4},{1,3},{3,1},{5,7},{7,5},{8,10},{10,8},{12,... | collective-permute-start | bytes 12296 | tf_op jit(solution)/shard_map/ppermute | solution.py:430
where the time goes:
time: 68 us; the launch traced here: 67.9 us
  Pallas kernels  24.7 us (36%)
  waiting for transfers between devices  21.7 us (32%)
  starting transfers between devices  20.4 us (30%)
  between operations  0.94 us (1%)
    pallas_call x13, Pallas kernels, call(): pl.pallas_call(kernel, out_shape=placed, in_specs=spaces, out_specs=out_s...  23.9 us
    ppermute x9, starting transfers between devices, shifted(): out.append(lax.ppermute(x, axis, pairs))  17.8 us
    ppermute x9, waiting for transfers between devices, shifted(): out.append(lax.ppermute(x, axis, pairs))  13.4 us
    ppermute x10, waiting for transfers between devices, swap(): return lax.ppermute(x, 'rep', SWAP)  8.29 us
    ppermute x10, starting transfers between devices, swap(): return lax.ppermute(x, 'rep', SWAP)  2.65 us
  transfers between devices with their start and end apart: 19, of which 8 were waited for; matrix products, arithmetic and copies ran while one was open for 0% of the time, Pallas kernels for 27%

commit v1 on v0

--- a/solution.py
+++ b/solution.py
@@ -70,26 +70,10 @@
     return call(kernel, arrays, outs, [HBM] * n, [VMEM] * n, [pltpu.SemaphoreType.DMA((n,))], cost=1 << 21)
 
 
-def own_halves(arrays):
-    n = len(arrays)
-
-    def kernel(*refs):
-        me = lax.axis_index("rep")
-        sem = refs[-1]
-        pairs = []
-        for source, target in zip(refs[:n], refs[n : 2 * n]):
-            h = target.shape[0]
-            at = pl.ds(pl.multiple_of(me * h, 8), h)
-            pairs.append((source.at[0, at] if len(source.shape) == 3 else source.at[at], target))
-        copies(pairs, sem)
-
-    outs = [struct(a.shape[-2] // 2, a.shape[-1]) for a in arrays]
-    return call(kernel, arrays, outs, [HBM] * n, [VMEM] * n, [pltpu.SemaphoreType.DMA((n,))], cost=1 << 22)
-
-
 class Places:
     def __init__(self, heights, widths):
         self.halves = [h // 2 for h in heights]
+        self.widths = widths
         self.blocks = [up_to(h, LANES) // LANES for h in self.halves]
         self.tiles = [w // LANES for w in widths]
         self.row_at = [sum(self.blocks[:k]) for k in range(4)]
@@ -99,51 +83,89 @@
         self.n_column = up_to(self.spare + 1, 8)
 
 
+def accumulate(k, places, g_ref, m_ref, r_ref, own_ref, out_ref, partial):
+    h, n_blocks, tiles = places.halves[k], places.blocks[k], places.tiles[k]
+    row_at, column_at = places.row_at[k], places.n_row + places.column_at[k]
+
+    def step(i, sums):
+        rows = pl.ds(pl.multiple_of(i * 8, 8), 8)
+        sums = list(sums)
+        by_row = None
+        for j in range(tiles):
+            at = (rows, pl.ds(j * LANES, LANES))
+            grad = g_ref[at] + r_ref[at]
+            own_ref[at] = momentum_decay * m_ref[at] + (1.0 - momentum_decay) * grad
+            square = grad * grad
+            sums[j] = sums[j] + square
+            by_row = square if by_row is None else by_row + square
+        partial[rows, :] = by_row
+        return tuple(sums)
+
+    zero = jnp.zeros((8, LANES), jnp.float32)
+    sums = lax.fori_loop(0, h // 8, step, (zero,) * tiles, unroll=4)
+    for j in range(tiles):
+        out_ref[pl.ds(column_at + j, 1), :] = jnp.sum(sums[j], axis=0, keepdims=True)
+    if n_blocks * LANES > h:
+        partial[pl.ds(h, n_blocks * LANES - h), :] = jnp.zeros((n_blocks * LANES - h, LANES), jnp.float32)
+    for b in range(n_blocks):
+        turned = partial[pl.ds(b * LANES, LANES), :].T
+        out_ref[pl.ds(row_at + b, 1), :] = jnp.sum(turned, axis=0, keepdims=True)
+
+
+def own_halves(places, partials, momenta, received):
+    first, later = ORDER[0], ORDER[1:]
+    h, width = places.halves[first], places.widths[first]
+
+    def kernel(*refs):
+        me = lax.axis_index("rep")
+        g_refs, m_refs, r_ref = refs[:4], refs[4:8], refs[8]
+        held = dict(zip(later, zip(refs[9:12], refs[12:15])))
+        own_ref, out_ref = refs[15:17]
+        held[first] = refs[17:19]
+        partial, sem = refs[19], refs[20]
+        started = []
+        for k in ORDER:
+            at = pl.ds(pl.multiple_of(me * places.halves[k], 8), places.halves[k])
+            for source, target in zip((g_refs[k].at[0, at], m_refs[k].at[at]), held[k]):
+                started.append(pltpu.make_async_copy(source, target, sem.at[len(started)]))
+                started[-1].start()
+        out_ref[...] = jnp.zeros_like(out_ref)
+        for item in started[:2]:
+            item.wait()
+        accumulate(first, places, *held[first], r_ref, own_ref, out_ref, partial)
+        for item in started[2:]:
+            item.wait()
+
+    halves = [struct(places.halves[k], places.widths[k]) for k in later]
+    out = call(
+        kernel,
+        [*partials, *momenta, received],
+        [*halves, *halves, struct(h, width), struct(places.n_row + places.n_column, LANES)],
+        [HBM] * 8 + [VMEM],
+        [VMEM] * 8,
+        [pltpu.VMEM((h, width), jnp.float32)] * 2
+        + [pltpu.VMEM((places.blocks[first] * LANES, LANES), jnp.float32), pltpu.SemaphoreType.DMA((8,))],
+        limit=(4 << 20) + 8 * h * width,
+        cost=1 << 22,
+    )
+    return dict(zip(later, zip(out[:3], out[3:6]))), out[6], out[7]
+
+
 def statistics(k, places, g, m, received, packed):
     h, width = g.shape
-    n_blocks, tiles = places.blocks[k], places.tiles[k]
-    row_at, column_at = places.row_at[k], places.n_row + places.column_at[k]
-
-    def kernel(*refs):
-        g_ref, m_ref, r_ref = refs[:3]
-        own_ref, out_ref, partial = refs[-3:]
-        if packed is None:
-            out_ref[...] = jnp.zeros_like(out_ref)
-
-        def step(i, sums):
-            rows = pl.ds(pl.multiple_of(i * 8, 8), 8)
-            sums = list(sums)
-            by_row = None
-            for j in range(tiles):
-                at = (rows, pl.ds(j * LANES, LANES))
-                grad = g_ref[at] + r_ref[at]
-                own_ref[at] = momentum_decay * m_ref[at] + (1.0 - momentum_decay) * grad
-                square = grad * grad
-                sums[j] = sums[j] + square
-                by_row = square if by_row is None else by_row + square
-            partial[rows, :] = by_row
-            return tuple(sums)
-
-        zero = jnp.zeros((8, LANES), jnp.float32)
-        sums = lax.fori_loop(0, h // 8, step, (zero,) * tiles, unroll=2)
-        for j in range(tiles):
-            out_ref[pl.ds(column_at + j, 1), :] = jnp.sum(sums[j], axis=0, keepdims=True)
-        if n_blocks * LANES > h:
-            partial[pl.ds(h, n_blocks * LANES - h), :] = jnp.zeros((n_blocks * LANES - h, LANES), jnp.float32)
-        for b in range(n_blocks):
-            turned = partial[pl.ds(b * LANES, LANES), :].T
-            out_ref[pl.ds(row_at + b, 1), :] = jnp.sum(turned, axis=0, keepdims=True)
-
-    ins = [g, m, received] + ([] if packed is None else [packed])
+
+    def kernel(g_ref, m_ref, r_ref, packed_ref, own_ref, out_ref, partial):
+        accumulate(k, places, g_ref, m_ref, r_ref, own_ref, out_ref, partial)
+
     return call(
         kernel,
-        ins,
-        [struct(h, width), struct(places.n_row + places.n_column, LANES)],
-        [VMEM] * len(ins),
+        [g, m, received, packed],
+        [struct(h, width), struct(*packed.shape)],
+        [VMEM] * 4,
         [VMEM, VMEM],
-        [pltpu.VMEM((n_blocks * LANES, LANES), jnp.float32)],
+        [pltpu.VMEM((places.blocks[k] * LANES, LANES), jnp.float32)],
         cost=1 << 20,
-        aliases=None if packed is None else {3: 1},
+        aliases={3: 1},
     )
 
 
@@ -153,7 +175,7 @@
         factor[pl.ds(b * LANES, LANES), :] = wide
 
 
-def shares(places, column_count, rows_old, row_parts, packed, own, after):
+def shares(places, column_count, rows_old, row_parts, packed, own, after, early=()):
     n_parts = len(row_parts)
 
     def old_rows(k, ref, me):
@@ -217,15 +239,15 @@
 
     return call(
         kernel,
-        [*rows_old, packed, *row_parts, *own, *after],
+        [*rows_old, packed, *row_parts, *own, *after, *early],
         [struct(places.n_row, LANES), struct(sum(places.blocks) * LANES, LANES), struct(2 * places.n_column, LANES)],
-        [VMEM] * (9 + n_parts) + [HBM] * len(after),
+        [VMEM] * (9 + n_parts) + [HBM] * len(after) + [VMEM] * len(early),
         [VMEM] * 3,
         cost=1 << 21,
     )
 
 
-def columns(places, row_count, columns_old, total, other, after):
+def columns(places, row_count, columns_old, total, other, after, early=()):
     def kernel(c0, c1, c2, c3, total_ref, other_ref, *rest):
         columns_out, out_ref = rest[-2:]
         old_refs = (c0, c1, c2, c3)
@@ -245,116 +267,92 @@
 
     return call(
         kernel,
-        [*columns_old, total, other, *after],
+        [*columns_old, total, other, *after, *early],
         [struct(places.n_column, LANES), struct(8, LANES)],
-        [VMEM] * 6 + [HBM] * len(after),
+        [VMEM] * 6 + [HBM] * len(after) + [VMEM] * len(early),
         [VMEM] * 2,
         cost=1 << 20,
     )
 
 
-def load_weights(weights, after):
-    n = len(weights)
-
-    def kernel(*refs):
-        copies(list(zip(refs[:n], refs[n + 1 : 2 * n + 1])), refs[-1])
-
-    return call(
-        kernel,
-        [*weights, after],
-        [struct(*w.shape) for w in weights],
-        [HBM] * n + [VMEM],
-        [VMEM] * n,
-        [pltpu.SemaphoreType.DMA((n,))],
-        cost=1 << 24,
-    )
-
-
-def write_own(own, shapes, weights, after):
-    n = len(weights)
-
-    def kernel(*refs):
-        me = lax.axis_index("rep")
-        outs = refs[5 + n :]
-        pairs = list(zip(refs[5 : 5 + n], outs[4 : 4 + n]))
-        for k in range(4):
-            h = refs[k].shape[0]
-            pairs.append((refs[k], outs[k].at[pl.ds(pl.multiple_of(me * h, 8), h)]))
-        copies(pairs, refs[-1])
-
-    out = call(
-        kernel,
-        [*own, after, *weights],
-        shapes + [struct(*w.shape) for w in weights],
-        [VMEM] * 5 + [HBM] * n,
-        [HBM] * 4 + [VMEM] * n,
-        [pltpu.SemaphoreType.DMA((4 + n,))],
-        cost=1 << 24,
-    )
-    return out[:4], out[4:]
-
-
-def write_back(back, momenta):
+def write_own(own, shapes, after, early=()):
     def kernel(*refs):
         me = lax.axis_index("rep")
         pairs = []
         for k in range(4):
             h = refs[k].shape[0]
-            pairs.append((refs[k], refs[8 + k].at[pl.ds(pl.multiple_of((1 - me) * h, 8), h)]))
+            pairs.append((refs[k], refs[5 + len(early) + k].at[pl.ds(pl.multiple_of(me * h, 8), h)]))
         copies(pairs, refs[-1])
 
     return call(
         kernel,
-        [*back, *momenta],
-        [struct(*m.shape) for m in momenta],
-        [VMEM] * 4 + [HBM] * 4,
+        [*own, after, *early],
+        shapes,
+        [VMEM] * (5 + len(early)),
         [HBM] * 4,
         [pltpu.SemaphoreType.DMA((4,))],
         cost=1 << 24,
-        aliases={4 + k: k for k in range(4)},
-    )
-
-
-def write_moments(places, rows_own, rows_other, columns_new):
+    )
+
+
+def write_back(places, back, momenta, rows_own, rows_other, columns_new):
     counts = [2 * h // LANES for h in places.halves]
 
-    def kernel(own_ref, other_ref, columns_ref, *outs):
+    def kernel(*refs):
         me = lax.axis_index("rep")
-        row_refs, column_refs = outs[:4], outs[4:8]
-        spread_rows(lax.rsqrt(other_ref[...]), outs[8], sum(places.blocks))
+        own_ref, other_ref, columns_ref = refs[8:11]
+        outs, small, factor = refs[11:15], refs[15:23], refs[23]
+        stages, sem = refs[24:32], refs[32]
+        started = []
+
+        def begin(source, target):
+            started.append(pltpu.make_async_copy(source, target, sem.at[len(started)]))
+            started[-1].start()
+
+        for k in range(4):
+            h = refs[k].shape[0]
+            begin(refs[k], outs[k].at[pl.ds(pl.multiple_of((1 - me) * h, 8), h)])
         for k in range(4):
             h, n = places.halves[k], places.blocks[k]
-            column_refs[k][...] = columns_ref[pl.ds(places.column_at[k], places.tiles[k]), :]
+            row_ref, column_ref = stages[k], stages[4 + k]
+            column_ref[...] = columns_ref[pl.ds(places.column_at[k], places.tiles[k]), :]
             mine = own_ref[pl.ds(places.row_at[k], n), :]
             other = other_ref[pl.ds(places.row_at[k], n), :]
             first = jnp.where(me == 0, mine, other)
             second = jnp.where(me == 0, other, mine)
             whole, rest = divmod(h, LANES)
             if not rest:
-                row_refs[k][pl.ds(0, n), :] = first
-                row_refs[k][pl.ds(n, n), :] = second
-                continue
-            turned = pltpu.roll(second, rest, 1)
-            low = lax.broadcasted_iota(jnp.int32, (1, LANES), 1) < rest
-            row_refs[k][pl.ds(0, whole), :] = first[:whole]
-            before = first[whole : whole + 1]
-            for i in range(counts[k] - whole):
-                here = turned[i : i + 1]
-                row_refs[k][pl.ds(whole + i, 1), :] = jnp.where(low, before, here)
-                before = here
-
-    ins = [pltpu.with_memory_space_constraint(x, pltpu.VMEM) for x in (rows_own, rows_other, columns_new)]
-    out = pl.pallas_call(
-        kernel,
-        name="write_moments",
-        out_shape=[struct(n, LANES) for n in counts + places.tiles]
-        + [pltpu.VMEM((sum(places.blocks) * LANES, LANES), jnp.float32)],
-        in_specs=[VMEM] * 3,
-        out_specs=[VMEM] * 9,
-        compiler_params=pltpu.CompilerParams(vmem_limit_bytes=2 << 20),
-        cost_estimate=pl.CostEstimate(flops=1 << 24, bytes_accessed=0, transcendentals=0),
-    )(*ins)
-    return out[:4], out[4:8], out[8]
+                row_ref[pl.ds(0, n), :] = first
+                row_ref[pl.ds(n, n), :] = second
+            else:
+                turned = pltpu.roll(second, rest, 1)
+                low = lax.broadcasted_iota(jnp.int32, (1, LANES), 1) < rest
+                row_ref[pl.ds(0, whole), :] = first[:whole]
+                before = first[whole : whole + 1]
+                for i in range(counts[k] - whole):
+                    here = turned[i : i + 1]
+                    row_ref[pl.ds(whole + i, 1), :] = jnp.where(low, before, here)
+                    before = here
+            begin(row_ref, small[k])
+            begin(column_ref, small[4 + k])
+        spread_rows(lax.rsqrt(other_ref[...]), factor, sum(places.blocks))
+        for item in started:
+            item.wait()
+
+    sizes = counts + places.tiles
+    out = call(
+        kernel,
+        [*back, *momenta, rows_own, rows_other, columns_new],
+        [struct(*m.shape) for m in momenta]
+        + [struct(n, LANES) for n in sizes]
+        + [struct(sum(places.blocks) * LANES, LANES)],
+        [VMEM] * 4 + [HBM] * 4 + [VMEM] * 3,
+        [HBM] * 12 + [VMEM],
+        [pltpu.VMEM((n, LANES), jnp.float32) for n in sizes] + [pltpu.SemaphoreType.DMA((12,))],
+        cost=1 << 24,
+        aliases={4 + k: k for k in range(4)},
+    )
+    return out[:4], out[4:8], out[8:12], out[12]
 
 
 def write_weights(places, row_count, column_count, n_share, masses, factors, columns_new, own, back, weights, outs):
@@ -445,29 +443,29 @@
     for group in (ORDER[:1], ORDER[1:]):
         for k, other in zip(group, other_halves([partials[k] for k in group])):
             received[k] = swap(other)
-    halves = own_halves([*partials, *momenta])
     rows_old = [item.reshape(-1, LANES) for item in rows]
     columns_old = [item.reshape(-1, LANES) for item in columns_in]
-    own, back, packed = [None] * 4, [None] * 4, None
+    own, back = [None] * 4, [None] * 4
+    halves, own[ORDER[0]], packed = own_halves(places, partials, momenta, received[ORDER[0]])
+    for k in ORDER[1:]:
+        own[k], packed = statistics(k, places, *halves[k], received[k], packed)
     for k in ORDER:
-        own[k], packed = statistics(k, places, halves[k], halves[4 + k], received[k], packed)
         back[k] = swap(own[k])
 
     row_parts = shifted(packed[: places.n_row], "tp")
-    held_first = load_weights([weights[0], weights[3]], packed)
-    rows_own, factor_own, local = shares(places, column_count, rows_old, row_parts, packed, own, ())
+    rows_own, factor_own, local = shares(places, column_count, rows_old, row_parts, packed, own, (), weights)
 
     rows_other = swap(rows_own)
     total = sum(shifted(local, "fs"), local)
-    momenta_next, held_second = write_own(own, shapes, [weights[1], weights[2]], local)
-    momenta_next = write_back(back, momenta_next)
+    momenta_next = write_own(own, shapes, local)
     columns_new, mass = columns(places, row_count, columns_old, total, swap(total), ())
 
-    held = [held_first[0], *held_second, held_first[1]]
     masses = [mass, *shifted(mass, "tp")]
-    rows_new, columns_out, factor_other = write_moments(places, rows_own, rows_other, columns_new)
+    momenta_next, rows_new, columns_out, factor_other = write_back(
+        places, back, momenta_next, rows_own, rows_other, columns_new
+    )
     weights_next = write_weights(
-        places, row_count, column_count, n_tp, masses, [factor_own, factor_other], columns_new, own, back, held, shapes
+        places, row_count, column_count, n_tp, masses, [factor_own, factor_other], columns_new, own, back, weights, shapes
     )
     out = []
     for k in range(4):

time: 68 us -> 63.5 us (0.934)
  Pallas kernels: 24.7 us -> 18.9 us
  starting transfers between devices: 20.4 us -> 22.7 us
  waiting for transfers between devices: 21.7 us -> 20.7 us
    pallas_call x13 -> x11, Pallas kernels: 23.9 us -> 18.9 us  [call(): pl.pallas_call(kernel, out_shape=placed, in_specs=spaces, out_specs=out_s...]
    ppermute x9, waiting for transfers between devices: 13.4 us -> 11.2 us  [shifted(): out.append(lax.ppermute(x, axis, pairs))]
    ppermute x9, starting transfers between devices: 17.8 us -> 19.8 us  [shifted(): out.append(lax.ppermute(x, axis, pairs))]
    ppermute x10, waiting for transfers between devices: 8.29 us -> 9.51 us  [swap(): return lax.ppermute(x, 'rep', SWAP)]
    pallas_call x1 -> x0, Pallas kernels: 0.82 us -> none  [write_moments(): pl.pallas_call(kernel, name='write_moments', out_shape=[struct(n, LANES)...]
  transfers between devices with their start and end apart: 19 -> 19, of which waited for: 8 -> 10; matrix products, arithmetic and copies ran while one was open for 0% -> 0% of each run, Pallas kernels for 27% -> 20%
where the time goes in v1:
time: 63.5 us; the launch traced here: 63.4 us
  starting transfers between devices  22.7 us (36%)
  waiting for transfers between devices  20.7 us (33%)
  Pallas kernels  18.9 us (30%)
  between operations  0.95 us (1%)
    ppermute x9, starting transfers between devices, shifted(): out.append(lax.ppermute(x, axis, pairs))  19.8 us
    pallas_call x11, Pallas kernels, call(): pl.pallas_call(kernel, out_shape=placed, in_specs=spaces, out_specs=out_s...  18.9 us
    ppermute x9, waiting for transfers between devices, shifted(): out.append(lax.ppermute(x, axis, pairs))  11.2 us
    ppermute x10, waiting for transfers between devices, swap(): return lax.ppermute(x, 'rep', SWAP)  9.51 us
    ppermute x10, starting transfers between devices, swap(): return lax.ppermute(x, 'rep', SWAP)  2.89 us
  transfers between devices with their start and end apart: 19, of which 10 were waited for; matrix products, arithmetic and copies ran while one was open for 0% of the time, Pallas kernels for 20%

profile of v1, /device:TPU:0, one launch (start us, length us, event | category | flops | bytes accessed | tf_op | source)
XLA Modules:
  0.0 63.4 jit_solution(15852511079234196853)
XLA Ops:
  0.6 1.4 %shard_map.315 = f32[256,1408]{1,0:T(8,128)S(1)} custom-call(f32[1,512,1408]{2,1,0:T(8,128)} %refs_0_.4), custom_call_target="tpu_custom_call" | custom-call | flops 2097152 | tf_op jit(solution)/shard_map/pallas_call | solution.py:34
  2.0 0.6 collective-permute-start
  2.6 1.9 %shard_map.317 = (f32[256,1408]{1,0:T(8,128)S(1)}, f32[704,512]{1,0:T(8,128)S(1)}, f32[256,512]{1,0:T(8,128)S(1)}) custom-call(f32[1,512,1408]{2,1,0:T(8,128)} %refs_0_.5, f32[1,1408,512]{2,1,0:T(8,128)} %refs_1_.3, f32[1,512,512]{2,1,0:T(8,128)} %refs_2_.3), custom_call_target="tpu_custom_call" | custom-call | flops 2097152 | tf_op jit(solution)/shard_map/pallas_call | solution.py:34
  4.5 0.1 collective-permute-start.3
  4.6 0.5 collective-permute-start.2
  5.1 0.3 collective-permute-done.refs_8_
  5.4 3.8 %shard_map.316 = (f32[256,1408]{1,0:T(8,128)S(1)}, f32[704,512]{1,0:T(8,128)S(1)}, f32[256,512]{1,0:T(8,128)S(1)}, f32[256,1408]{1,0:T(8,128)S(1)}, f32[704,512]...) custom-call(f32[1,512,1408]{2,1,0:T(8,128)} %refs_0_.4, ...), custom_call_target="tpu_custom_call" | custom-call | flops 4194304 | tf_op jit(solution)/shard_map/pallas_call | solution.py:34
  9.3 0.0 collective-permute-done.3.r_ref
  9.3 0.0 copy-start.2
  9.3 0.0 copy-start.3
  9.3 0.6 shard_map.318
  9.9 0.0 collective-permute-done.2.r_ref
  10.0 0.0 copy-start
  10.0 0.0 copy-start.1
  10.0 0.0 copy-start.4
  10.0 0.0 copy-start.7
  10.0 0.0 copy-start.8
  10.0 0.0 copy-start.9
  10.0 0.7 %shard_map.319 = (f32[704,512]{1,0:T(8,128)S(1)}, f32[48,128]{1,0:T(8,128)S(1)}) custom-call(f32[704,512]{1,0:T(8,128)S(1)} %get-tuple-element.62.g_ref, f32[704,512]{1,0:T(8,128)S(1)} %get-tuple-element.63.m_ref, f32[704,512]{1,0:T(8,128)S(1)} %collective-permute-done.2.r_ref, ...), custom_call_target="tpu_custom_call", output_to_operand_aliasing={{1}: (3, {})} | custom-call | flops 1048576 | tf_op jit(solution)/shard_map/pallas_call | solution.py:34
  10.7 0.5 collective-permute-start.16
  11.2 0.1 collective-permute-start.15
  11.3 0.4 collective-permute-start.14
  11.7 0.1 collective-permute-start.1
  11.8 7.1 %collective-permute-done.1.r_ref = f32[256,512]{1,0:T(8,128)S(1)} collective-permute-done((f32[256,512]{1,0:T(8,128)S(1)}, f32[256,512]{1,0:T(8,128)S(1)}, u32[]{:S(2)}, u32[]{:S(2)}) %collective-permute-start.1) | collective-permute-done | bytes 524320 | tf_op jit(solution)/shard_map/ppermute | solution.py:47
  18.9 0.3 shard_map.320
  19.2 0.4 collective-permute-start.17
  19.6 2.6 %collective-permute-start.4 = (f32[16,128]{1,0:T(8,128)S(1)}, f32[16,128]{1,0:T(8,128)S(1)}, u32[]{:S(2)}, u32[]{:S(2)}) collective-permute-start(f32[16,128]{1,0:T(8,128)S(1)} %slice.3), channel_id=1, source_target_pairs={{0,2},{2,0},{4,6},{6,4},{1,3},{3,1},{5,7},{7,5},{8,10},{10,8},{12,... | collective-permute-start | bytes 24584 | tf_op jit(solution)/shard_map/ppermute | solution.py:428
  22.2 1.6 %collective-permute-done.4.refs_5_ = f32[16,128]{1,0:T(8,128)S(1)} collective-permute-done((f32[16,128]{1,0:T(8,128)S(1)}, f32[16,128]{1,0:T(8,128)S(1)}, u32[]{:S(2)}, u32[]{:S(2)}) %collective-permute-start.4) | collective-permute-done | bytes 8224 | tf_op jit(solution)/shard_map/ppermute | solution.py:428
  23.9 2.1 %collective-permute-start.5 = (f32[16,128]{1,0:T(8,128)S(1)}, f32[16,128]{1,0:T(8,128)S(1)}, u32[]{:S(2)}, u32[]{:S(2)}) collective-permute-start(f32[16,128]{1,0:T(8,128)S(1)} %slice.3), channel_id=1, source_target_pairs={{0,4},{2,6},{4,0},{6,2},{1,5},{3,7},{5,1},{7,3},{8,12},{10,14},{12... | collective-permute-start | bytes 24584 | tf_op jit(solution)/shard_map/ppermute | solution.py:428
  25.9 1.6 %collective-permute-done.5.refs_6_ = f32[16,128]{1,0:T(8,128)S(1)} collective-permute-done((f32[16,128]{1,0:T(8,128)S(1)}, f32[16,128]{1,0:T(8,128)S(1)}, u32[]{:S(2)}, u32[]{:S(2)}) %collective-permute-start.5) | collective-permute-done | bytes 8224 | tf_op jit(solution)/shard_map/ppermute | solution.py:428
  27.6 3.0 %collective-permute-start.6 = (f32[16,128]{1,0:T(8,128)S(1)}, f32[16,128]{1,0:T(8,128)S(1)}, u32[]{:S(2)}, u32[]{:S(2)}) collective-permute-start(f32[16,128]{1,0:T(8,128)S(1)} %slice.3), channel_id=1, source_target_pairs={{0,6},{2,4},{4,2},{6,0},{1,7},{3,5},{5,3},{7,1},{8,14},{10,12},{12... | collective-permute-start | bytes 24584 | tf_op jit(solution)/shard_map/ppermute | solution.py:428
  30.5 1.6 %collective-permute-done.6.refs_7_ = f32[16,128]{1,0:T(8,128)S(1)} collective-permute-done((f32[16,128]{1,0:T(8,128)S(1)}, f32[16,128]{1,0:T(8,128)S(1)}, u32[]{:S(2)}, u32[]{:S(2)}) %collective-permute-start.6) | collective-permute-done | bytes 8224 | tf_op jit(solution)/shard_map/ppermute | solution.py:428
  32.1 0.0 copy-done.2
  32.1 0.0 copy-done.3
  32.2 0.0 copy-start.5
  32.2 0.0 copy-start.6
  32.2 0.0 copy-start.10
  32.2 0.0 copy-start.11
  32.2 1.4 %shard_map.321 = (f32[16,128]{1,0:T(8,128)S(1)}, f32[1536,128]{1,0:T(8,128)S(1)}, f32[64,128]{1,0:T(8,128)S(1)}) custom-call(f32[4,128]{1,0:T(4,128)S(1)} %bitcast.19, f32[4,128]{1,0:T(4,128)S(1)} %bitcast.20, f32[11,128]{1,0:T(8,128)S(1)} %bitcast.16, f32[4,128]{1,0:T(4,128)S(1)} %bitcast.21, f32[48,128]{1,0:T(8,128)S(1)} %get-tuple-element.71.refs_4_, ...), custom_call_target="tpu_custom_call" | custom-call | flops 2097152 | tf_op jit(solution)/shard_map/pallas_call | solution.py:34
  33.6 2.1 %collective-permute-start.7 = (f32[64,128]{1,0:T(8,128)S(1)}, f32[64,128]{1,0:T(8,128)S(1)}, u32[]{:S(2)}, u32[]{:S(2)}) collective-permute-start(f32[64,128]{1,0:T(8,128)S(1)} %get-tuple-element.76.refs_4_), channel_id=1, source_target_pairs={{0,8},{8,0},{16,24},{24,16},{1,9},{9,1},{17,25},{25,17},{2,10},{10... | collective-permute-start | bytes 98312 | tf_op jit(solution)/shard_map/ppermute | solution.py:428
  35.8 2.2 %collective-permute-done.7 = f32[64,128]{1,0:T(8,128)S(1)} collective-permute-done((f32[64,128]{1,0:T(8,128)S(1)}, f32[64,128]{1,0:T(8,128)S(1)}, u32[]{:S(2)}, u32[]{:S(2)}) %collective-permute-start.7) | collective-permute-done | bytes 32800 | tf_op jit(solution)/shard_map/ppermute | solution.py:428
  38.0 2.7 %collective-permute-start.8 = (f32[64,128]{1,0:T(8,128)S(1)}, f32[64,128]{1,0:T(8,128)S(1)}, u32[]{:S(2)}, u32[]{:S(2)}) collective-permute-start(f32[64,128]{1,0:T(8,128)S(1)} %get-tuple-element.76.refs_4_), channel_id=1, source_target_pairs={{0,16},{8,24},{16,0},{24,8},{1,17},{9,25},{17,1},{25,9},{2,18},{10... | collective-permute-start | bytes 98312 | tf_op jit(solution)/shard_map/ppermute | solution.py:428
  40.7 2.2 %collective-permute-done.8 = f32[64,128]{1,0:T(8,128)S(1)} collective-permute-done((f32[64,128]{1,0:T(8,128)S(1)}, f32[64,128]{1,0:T(8,128)S(1)}, u32[]{:S(2)}, u32[]{:S(2)}) %collective-permute-start.8) | collective-permute-done | bytes 32800 | tf_op jit(solution)/shard_map/ppermute | solution.py:428
  42.9 3.9 %collective-permute-start.9 = (f32[64,128]{1,0:T(8,128)S(1)}, f32[64,128]{1,0:T(8,128)S(1)}, u32[]{:S(2)}, u32[]{:S(2)}) collective-permute-start(f32[64,128]{1,0:T(8,128)S(1)} %get-tuple-element.76.refs_4_), channel_id=1, source_target_pairs={{0,24},{8,16},{16,8},{24,0},{1,25},{9,17},{17,9},{25,1},{2,26},{10... | collective-permute-start | bytes 98312 | tf_op jit(solution)/shard_map/ppermute | solution.py:428
  46.8 1.9 %collective-permute-done.9 = f32[64,128]{1,0:T(8,128)S(1)} collective-permute-done((f32[64,128]{1,0:T(8,128)S(1)}, f32[64,128]{1,0:T(8,128)S(1)}, u32[]{:S(2)}, u32[]{:S(2)}) %collective-permute-start.9) | collective-permute-done | bytes 32800 | tf_op jit(solution)/shard_map/ppermute | solution.py:428
  48.7 0.1 collective-permute-start.10
  48.8 1.2 %collective-permute-done.10.other_ref = f32[64,128]{1,0:T(8,128)S(1)} collective-permute-done((f32[64,128]{1,0:T(8,128)S(1)}, f32[64,128]{1,0:T(8,128)S(1)}, u32[]{:S(2)}, u32[]{:S(2)}) %collective-permute-start.10) | collective-permute-done | bytes 32800 | tf_op jit(solution)/shard_map/ppermute | solution.py:47
  50.0 0.2 collective-permute-start.18
  50.1 0.0 copy-done.10
  50.1 0.1 shard_map.322
  50.3 0.8 %collective-permute-done.18.refs_9_ = f32[16,128]{1,0:T(8,128)S(1)} collective-permute-done((f32[16,128]{1,0:T(8,128)S(1)}, f32[16,128]{1,0:T(8,128)S(1)}, u32[]{:S(2)}, u32[]{:S(2)}) %collective-permute-start.18) | collective-permute-done | bytes 8224 | tf_op jit(solution)/shard_map/ppermute | solution.py:47
  51.1 1.5 %collective-permute-start.11 = (f32[8,128]{1,0:T(8,128)S(1)}, f32[8,128]{1,0:T(8,128)S(1)}, u32[]{:S(2)}, u32[]{:S(2)}) collective-permute-start(f32[8,128]{1,0:T(8,128)S(1)} %get-tuple-element.77.refs_0_), channel_id=1, source_target_pairs={{0,2},{2,0},{4,6},{6,4},{1,3},{3,1},{5,7},{7,5},{8,10},{10,8},{12,... | collective-permute-start | bytes 12296 | tf_op jit(solution)/shard_map/ppermute | solution.py:428
  52.6 0.0 collective-permute-done.17.refs_3_.refs_14_
  52.6 1.5 %collective-permute-start.12 = (f32[8,128]{1,0:T(8,128)S(1)}, f32[8,128]{1,0:T(8,128)S(1)}, u32[]{:S(2)}, u32[]{:S(2)}) collective-permute-start(f32[8,128]{1,0:T(8,128)S(1)} %get-tuple-element.77.refs_0_), channel_id=1, source_target_pairs={{0,4},{2,6},{4,0},{6,2},{1,5},{3,7},{5,1},{7,3},{8,12},{10,14},{12... | collective-permute-start | bytes 12296 | tf_op jit(solution)/shard_map/ppermute | solution.py:428
  54.2 0.0 collective-permute-done.16.refs_2_.refs_13_
  54.2 0.5 collective-permute-start.13
  54.6 2.2 %shard_map.323 = (f32[512,1408]{1,0:T(8,128)}, f32[512,1408]{1,0:T(8,128)}, f32[1408,512]{1,0:T(8,128)}, f32[512,512]{1,0:T(8,128)}) custom-call(f32[256,1408]{1,0:T(8,128)S(1)} %get-tuple-element.72.refs_8_.refs_0_.refs_7_, f32[256,1408]{1,0:T(8,128)S(1)} %get-tuple-element.73.refs_9_.refs_1_.refs_8_, ...), custom_call_target="tpu_custom_call" | custom-call | flops 16777216 | tf_op jit(solution)/shard_map/pallas_call | solution.py:34
  56.9 0.0 collective-permute-done.15.refs_1_.refs_12_
  56.9 0.0 collective-permute-done.14.refs_0_.refs_11_
  56.9 2.4 %shard_map.324 = (f32[512,1408]{1,0:T(8,128)}, f32[512,1408]{1,0:T(8,128)}, f32[1408,512]{1,0:T(8,128)}, f32[512,512]{1,0:T(8,128)}, f32[4,128]{1,0:T(4,128)}, /...) custom-call(f32[256,1408]{1,0:T(8,128)S(1)} %collective-permute-done, ...), custom_call_target="tpu_custom_call", output_to_operand_aliasing={{0}: (4, {}), {1}: (5, {}), {2}: (6, {}), {3}: (7, {})} | custom-call | flops 16777216 | tf_op jit(solution)/shard_map/pallas_call | solution.py:34
  59.3 0.0 collective-permute-done.11.refs_1_
  59.3 0.0 collective-permute-done.12.refs_2_
  59.3 0.0 collective-permute-done.13.refs_3_
  59.3 4.1 %shard_map.325 = (f32[512,1408]{1,0:T(8,128)}, f32[512,1408]{1,0:T(8,128)}, f32[1408,512]{1,0:T(8,128)}, f32[512,512]{1,0:T(8,128)}) custom-call(f32[8,128]{1,0:T(8,128)S(1)} %get-tuple-element.77.refs_0_, f32[8,128]{1,0:T(8,128)S(1)} %collective-permute-done.11.refs_1_, f32[8,128]{1,0:T(8,128)S(1)} %collective-permute-done.12.refs_2_, ...), custom_call_target="tpu_custom_call" | custom-call | flops 4194304 | tf_op jit(solution)/shard_map/pallas_call | solution.py:34
  (11 shorter events, 0.0 us)
Async XLA Ops:
  2.0 3.4 %collective-permute-start = (f32[256,1408]{1,0:T(8,128)S(1)}, f32[256,1408]{1,0:T(8,128)S(1)}, u32[]{:S(2)}, u32[]{:S(2)}) collective-permute-start(f32[256,1408]{1,0:T(8,128)S(1)} %shard_map.315), channel_id=1, source_target_pairs={{0,1},{1,0},{2,3},{3,2},{4,5},{5,4},{6,7},{7,6},{8,9},{9,8},{10,11... | collective-permute-start | bytes 4325384 | tf_op jit(solution)/shard_map/ppermute | solution.py:47
  4.5 4.8 %collective-permute-start.3 = (f32[256,1408]{1,0:T(8,128)S(1)}, f32[256,1408]{1,0:T(8,128)S(1)}, u32[]{:S(2)}, u32[]{:S(2)}) collective-permute-start(f32[256,1408]{1,0:T(8,128)S(1)} %get-tuple-element.67), channel_id=1, source_target_pairs={{0,1},{1,0},{2,3},{3,2},{4,5},{5,4},{6,7},{7,6},{8,9},{9,8},{10,11... | collective-permute-start | bytes 4325384 | tf_op jit(solution)/shard_map/ppermute | solution.py:47
  4.6 5.3 %collective-permute-start.2 = (f32[704,512]{1,0:T(8,128)S(1)}, f32[704,512]{1,0:T(8,128)S(1)}, u32[]{:S(2)}, u32[]{:S(2)}) collective-permute-start(f32[704,512]{1,0:T(8,128)S(1)} %get-tuple-element.64), channel_id=1, source_target_pairs={{0,1},{1,0},{2,3},{3,2},{4,5},{5,4},{6,7},{7,6},{8,9},{9,8},{10,11... | collective-permute-start | bytes 4325384 | tf_op jit(solution)/shard_map/ppermute | solution.py:47
  9.3 22.8 %copy-start.2 = (f32[1408,512]{1,0:T(8,128)S(1)}, f32[1408,512]{1,0:T(8,128)}, u32[]{:S(2)}) copy-start(f32[1408,512]{1,0:T(8,128)} %refs_17_.1) | copy-start | bytes 8650756
  9.3 22.8 %copy-start.3 = (f32[512,512]{1,0:T(8,128)S(1)}, f32[512,512]{1,0:T(8,128)}, u32[]{:S(2)}) copy-start(f32[512,512]{1,0:T(8,128)} %refs_18_.1) | copy-start | bytes 3145732
  10.0 22.2 %copy-start = (f32[512,1408]{1,0:T(8,128)S(1)}, f32[512,1408]{1,0:T(8,128)}, u32[]{:S(2)}) copy-start(f32[512,1408]{1,0:T(8,128)} %refs_15_.3) | copy-start | bytes 8650756
  10.0 22.2 %copy-start.1 = (f32[512,1408]{1,0:T(8,128)S(1)}, f32[512,1408]{1,0:T(8,128)}, u32[]{:S(2)}) copy-start(f32[512,1408]{1,0:T(8,128)} %refs_16_.1) | copy-start | bytes 8650756
  10.0 22.2 %copy-start.4 = (f32[1408]{0:T(1024)S(1)}, f32[1408]{0:T(1024)}, u32[]{:S(2)}) copy-start(f32[1408]{0:T(1024)} %param.33) | copy-start | bytes 16900
  10.0 22.2 %copy-start.7 = (f32[512]{0:T(512)S(1)}, f32[512]{0:T(512)}, u32[]{:S(2)}) copy-start(f32[512]{0:T(512)} %param.23) | copy-start | bytes 6148
  10.0 22.2 %copy-start.8 = (f32[512]{0:T(512)S(1)}, f32[512]{0:T(512)}, u32[]{:S(2)}) copy-start(f32[512]{0:T(512)} %param.28) | copy-start | bytes 6148
  10.0 22.2 %copy-start.9 = (f32[512]{0:T(512)S(1)}, f32[512]{0:T(512)}, u32[]{:S(2)}) copy-start(f32[512]{0:T(512)} %param.38) | copy-start | bytes 6148
  10.7 43.5 %collective-permute-start.16 = (f32[704,512]{1,0:T(8,128)S(1)}, f32[704,512]{1,0:T(8,128)S(1)}, u32[]{:S(2)}, u32[]{:S(2)}) collective-permute-start(f32[704,512]{1,0:T(8,128)S(1)} %get-tuple-element.74.refs_10_.refs_2_.refs_9_), channel_id=1, source_target_pairs={{0,1},{1,0},{2,3},{3,2},{4,5},{5,4},{6,7},{7,6},{8,9},{9,8},{10,11... | collective-permute-start | bytes 4325384 | tf_op jit(solution)/shard_map/ppermute | solution.py:47
  11.2 45.7 %collective-permute-start.15 = (f32[256,1408]{1,0:T(8,128)S(1)}, f32[256,1408]{1,0:T(8,128)S(1)}, u32[]{:S(2)}, u32[]{:S(2)}) collective-permute-start(f32[256,1408]{1,0:T(8,128)S(1)} %get-tuple-element.73.refs_9_.refs_1_.refs_8_), channel_id=1, source_target_pairs={{0,1},{1,0},{2,3},{3,2},{4,5},{5,4},{6,7},{7,6},{8,9},{9,8},{10,11... | collective-permute-start | bytes 4325384 | tf_op jit(solution)/shard_map/ppermute | solution.py:47
  11.3 45.6 %collective-permute-start.14 = (f32[256,1408]{1,0:T(8,128)S(1)}, f32[256,1408]{1,0:T(8,128)S(1)}, u32[]{:S(2)}, u32[]{:S(2)}) collective-permute-start(f32[256,1408]{1,0:T(8,128)S(1)} %get-tuple-element.72.refs_8_.refs_0_.refs_7_), channel_id=1, source_target_pairs={{0,1},{1,0},{2,3},{3,2},{4,5},{5,4},{6,7},{7,6},{8,9},{9,8},{10,11... | collective-permute-start | bytes 4325384 | tf_op jit(solution)/shard_map/ppermute | solution.py:47
  11.7 7.2 %collective-permute-start.1 = (f32[256,512]{1,0:T(8,128)S(1)}, f32[256,512]{1,0:T(8,128)S(1)}, u32[]{:S(2)}, u32[]{:S(2)}) collective-permute-start(f32[256,512]{1,0:T(8,128)S(1)} %get-tuple-element.61), channel_id=1, source_target_pairs={{0,1},{1,0},{2,3},{3,2},{4,5},{5,4},{6,7},{7,6},{8,9},{9,8},{10,11... | collective-permute-start | bytes 1572872 | tf_op jit(solution)/shard_map/ppermute | solution.py:47
  19.2 33.4 %collective-permute-start.17 = (f32[256,512]{1,0:T(8,128)S(1)}, f32[256,512]{1,0:T(8,128)S(1)}, u32[]{:S(2)}, u32[]{:S(2)}) collective-permute-start(f32[256,512]{1,0:T(8,128)S(1)} %get-tuple-element.75.refs_11_.refs_3_.refs_10_), channel_id=1, source_target_pairs={{0,1},{1,0},{2,3},{3,2},{4,5},{5,4},{6,7},{7,6},{8,9},{9,8},{10,11... | collective-permute-start | bytes 1572872 | tf_op jit(solution)/shard_map/ppermute | solution.py:47
  19.6 4.2 %collective-permute-start.4 = (f32[16,128]{1,0:T(8,128)S(1)}, f32[16,128]{1,0:T(8,128)S(1)}, u32[]{:S(2)}, u32[]{:S(2)}) collective-permute-start(f32[16,128]{1,0:T(8,128)S(1)} %slice.3), channel_id=1, source_target_pairs={{0,2},{2,0},{4,6},{6,4},{1,3},{3,1},{5,7},{7,5},{8,10},{10,8},{12,... | collective-permute-start | bytes 24584 | tf_op jit(solution)/shard_map/ppermute | solution.py:428
  23.9 3.7 %collective-permute-start.5 = (f32[16,128]{1,0:T(8,128)S(1)}, f32[16,128]{1,0:T(8,128)S(1)}, u32[]{:S(2)}, u32[]{:S(2)}) collective-permute-start(f32[16,128]{1,0:T(8,128)S(1)} %slice.3), channel_id=1, source_target_pairs={{0,4},{2,6},{4,0},{6,2},{1,5},{3,7},{5,1},{7,3},{8,12},{10,14},{12... | collective-permute-start | bytes 24584 | tf_op jit(solution)/shard_map/ppermute | solution.py:428
  27.6 4.6 %collective-permute-start.6 = (f32[16,128]{1,0:T(8,128)S(1)}, f32[16,128]{1,0:T(8,128)S(1)}, u32[]{:S(2)}, u32[]{:S(2)}) collective-permute-start(f32[16,128]{1,0:T(8,128)S(1)} %slice.3), channel_id=1, source_target_pairs={{0,6},{2,4},{4,2},{6,0},{1,7},{3,5},{5,3},{7,1},{8,14},{10,12},{12... | collective-permute-start | bytes 24584 | tf_op jit(solution)/shard_map/ppermute | solution.py:428
  32.2 17.9 %copy-start.5 = (f32[1408]{0:T(1024)S(1)}, f32[1408]{0:T(1024)}, u32[]{:S(2)}) copy-start(f32[1408]{0:T(1024)} %param.24) | copy-start | bytes 16900
  32.2 17.9 %copy-start.6 = (f32[1408]{0:T(1024)S(1)}, f32[1408]{0:T(1024)}, u32[]{:S(2)}) copy-start(f32[1408]{0:T(1024)} %param.29) | copy-start | bytes 16900
  32.2 17.9 %copy-start.10 = (f32[512]{0:T(512)S(1)}, f32[512]{0:T(512)}, u32[]{:S(2)}) copy-start(f32[512]{0:T(512)} %param.34) | copy-start | bytes 6148
  32.2 17.9 %copy-start.11 = (f32[512]{0:T(512)S(1)}, f32[512]{0:T(512)}, u32[]{:S(2)}) copy-start(f32[512]{0:T(512)} %param.39) | copy-start | bytes 6148
  33.6 4.3 %collective-permute-start.7 = (f32[64,128]{1,0:T(8,128)S(1)}, f32[64,128]{1,0:T(8,128)S(1)}, u32[]{:S(2)}, u32[]{:S(2)}) collective-permute-start(f32[64,128]{1,0:T(8,128)S(1)} %get-tuple-element.76.refs_4_), channel_id=1, source_target_pairs={{0,8},{8,0},{16,24},{24,16},{1,9},{9,1},{17,25},{25,17},{2,10},{10... | collective-permute-start | bytes 98312 | tf_op jit(solution)/shard_map/ppermute | solution.py:428
  38.0 4.9 %collective-permute-start.8 = (f32[64,128]{1,0:T(8,128)S(1)}, f32[64,128]{1,0:T(8,128)S(1)}, u32[]{:S(2)}, u32[]{:S(2)}) collective-permute-start(f32[64,128]{1,0:T(8,128)S(1)} %get-tuple-element.76.refs_4_), channel_id=1, source_target_pairs={{0,16},{8,24},{16,0},{24,8},{1,17},{9,25},{17,1},{25,9},{2,18},{10... | collective-permute-start | bytes 98312 | tf_op jit(solution)/shard_map/ppermute | solution.py:428
  42.9 5.8 %collective-permute-start.9 = (f32[64,128]{1,0:T(8,128)S(1)}, f32[64,128]{1,0:T(8,128)S(1)}, u32[]{:S(2)}, u32[]{:S(2)}) collective-permute-start(f32[64,128]{1,0:T(8,128)S(1)} %get-tuple-element.76.refs_4_), channel_id=1, source_target_pairs={{0,24},{8,16},{16,8},{24,0},{1,25},{9,17},{17,9},{25,1},{2,26},{10... | collective-permute-start | bytes 98312 | tf_op jit(solution)/shard_map/ppermute | solution.py:428
  48.7 1.3 %collective-permute-start.10 = (f32[64,128]{1,0:T(8,128)S(1)}, f32[64,128]{1,0:T(8,128)S(1)}, u32[]{:S(2)}, u32[]{:S(2)}) collective-permute-start(f32[64,128]{1,0:T(8,128)S(1)} %add_add_fusion.total_ref), channel_id=1, source_target_pairs={{0,1},{1,0},{2,3},{3,2},{4,5},{5,4},{6,7},{7,6},{8,9},{9,8},{10,11... | collective-permute-start | bytes 98312 | tf_op jit(solution)/shard_map/ppermute | solution.py:47
  50.0 1.2 %collective-permute-start.18 = (f32[16,128]{1,0:T(8,128)S(1)}, f32[16,128]{1,0:T(8,128)S(1)}, u32[]{:S(2)}, u32[]{:S(2)}) collective-permute-start(f32[16,128]{1,0:T(8,128)S(1)} %get-tuple-element.83.refs_8_), channel_id=1, source_target_pairs={{0,1},{1,0},{2,3},{3,2},{4,5},{5,4},{6,7},{7,6},{8,9},{9,8},{10,11... | collective-permute-start | bytes 24584 | tf_op jit(solution)/shard_map/ppermute | solution.py:47
  51.1 8.1 %collective-permute-start.11 = (f32[8,128]{1,0:T(8,128)S(1)}, f32[8,128]{1,0:T(8,128)S(1)}, u32[]{:S(2)}, u32[]{:S(2)}) collective-permute-start(f32[8,128]{1,0:T(8,128)S(1)} %get-tuple-element.77.refs_0_), channel_id=1, source_target_pairs={{0,2},{2,0},{4,6},{6,4},{1,3},{3,1},{5,7},{7,5},{8,10},{10,8},{12,... | collective-permute-start | bytes 12296 | tf_op jit(solution)/shard_map/ppermute | solution.py:428
  52.6 6.7 %collective-permute-start.12 = (f32[8,128]{1,0:T(8,128)S(1)}, f32[8,128]{1,0:T(8,128)S(1)}, u32[]{:S(2)}, u32[]{:S(2)}) collective-permute-start(f32[8,128]{1,0:T(8,128)S(1)} %get-tuple-element.77.refs_0_), channel_id=1, source_target_pairs={{0,4},{2,6},{4,0},{6,2},{1,5},{3,7},{5,1},{7,3},{8,12},{10,14},{12... | collective-permute-start | bytes 12296 | tf_op jit(solution)/shard_map/ppermute | solution.py:428
  54.2 5.1 %collective-permute-start.13 = (f32[8,128]{1,0:T(8,128)S(1)}, f32[8,128]{1,0:T(8,128)S(1)}, u32[]{:S(2)}, u32[]{:S(2)}) collective-permute-start(f32[8,128]{1,0:T(8,128)S(1)} %get-tuple-element.77.refs_0_), channel_id=1, source_target_pairs={{0,6},{2,4},{4,2},{6,0},{1,7},{3,5},{5,3},{7,1},{8,14},{10,12},{12... | collective-permute-start | bytes 12296 | tf_op jit(solution)/shard_map/ppermute | solution.py:428

commit v2 on v1

--- a/solution.py
+++ b/solution.py
@@ -13,7 +13,7 @@
 
 EVERY = ("fs", "tp", "rep")
 SWAP = [(0, 1), (1, 0)]
-ORDER = (0, 1, 2, 3)
+ORDER = (2, 0, 1, 3)
 LANES = 128
 PARTS = 2
 HBM = pl.BlockSpec(memory_space=pltpu.HBM)
@@ -231,7 +231,7 @@
                 return tuple(sums)
 
             zero = jnp.zeros((8, LANES), jnp.float32)
-            sums = lax.fori_loop(0, places.halves[k] // 8, step, (zero,) * places.tiles[k], unroll=2)
+            sums = lax.fori_loop(0, places.halves[k] // 8, step, (zero,) * places.tiles[k], unroll=8)
             for j in range(places.tiles[k]):
                 at = pl.ds(places.n_column + places.column_at[k] + j, 1)
                 out_ref[at, :] = jnp.sum(sums[j], axis=0, keepdims=True)
@@ -395,7 +395,7 @@
                             stages[k][pl.ds(far, 8), lanes] = w_refs[k][pl.ds(far, 8), lanes] - change
                         return carry
 
-                    lax.fori_loop(0, chunk // 8, step, 0, unroll=2)
+                    lax.fori_loop(0, chunk // 8, step, 0, unroll=4)
                     at = pl.ds(pl.multiple_of(which * h + begin, 8), chunk)
                     copy = pltpu.make_async_copy(stages[k].at[at], out_refs[k].at[at], sem.at[len(waits)])
                     copy.start()

time: 63.5 us -> 63.1 us (level)
  no operation moved by 1% of the time
where the time goes in v2:
time: 63.1 us; the launch traced here: 63 us
  starting transfers between devices  22.7 us (36%)
  waiting for transfers between devices  20.7 us (33%)
  Pallas kernels  18.5 us (29%)
  between operations  0.95 us (2%)
    ppermute x9, starting transfers between devices, shifted(): out.append(lax.ppermute(x, axis, pairs))  19.8 us
    pallas_call x11, Pallas kernels, call(): pl.pallas_call(kernel, out_shape=placed, in_specs=spaces, out_specs=out_s...  18.5 us
    ppermute x9, waiting for transfers between devices, shifted(): out.append(lax.ppermute(x, axis, pairs))  11.2 us
    ppermute x10, waiting for transfers between devices, swap(): return lax.ppermute(x, 'rep', SWAP)  9.51 us
    ppermute x10, starting transfers between devices, swap(): return lax.ppermute(x, 'rep', SWAP)  2.89 us
  transfers between devices with their start and end apart: 19, of which 10 were waited for; matrix products, arithmetic and copies ran while one was open for 0% of the time, Pallas kernels for 20%

profile of v2, /device:TPU:0, one launch (start us, length us, event | category | flops | bytes accessed | tf_op | source)
XLA Modules:
  0.0 63.0 jit_solution(10959554274997385985)
XLA Ops:
  0.6 1.4 %shard_map.315 = f32[704,512]{1,0:T(8,128)S(1)} custom-call(f32[1,1408,512]{2,1,0:T(8,128)} %refs_2_.2), custom_call_target="tpu_custom_call" | custom-call | flops 2097152 | tf_op jit(solution)/shard_map/pallas_call | solution.py:34
  2.0 0.6 collective-permute-start
  2.6 1.9 %shard_map.317 = (f32[256,1408]{1,0:T(8,128)S(1)}, f32[256,1408]{1,0:T(8,128)S(1)}, f32[256,512]{1,0:T(8,128)S(1)}) custom-call(f32[1,512,1408]{2,1,0:T(8,128)} %refs_0_.5, f32[1,512,1408]{2,1,0:T(8,128)} %refs_1_.3, f32[1,512,512]{2,1,0:T(8,128)} %refs_2_.3), custom_call_target="tpu_custom_call" | custom-call | flops 2097152 | tf_op jit(solution)/shard_map/pallas_call | solution.py:34
  4.5 0.1 collective-permute-start.3
  4.6 0.5 collective-permute-start.2
  5.1 0.3 collective-permute-done.refs_8_
  5.4 3.8 %shard_map.316 = (f32[256,1408]{1,0:T(8,128)S(1)}, f32[256,1408]{1,0:T(8,128)S(1)}, f32[256,512]{1,0:T(8,128)S(1)}, f32[256,1408]{1,0:T(8,128)S(1)}, f32[256,140...) custom-call(f32[1,512,1408]{2,1,0:T(8,128)} %refs_0_.5, ...), custom_call_target="tpu_custom_call" | custom-call | flops 4194304 | tf_op jit(solution)/shard_map/pallas_call | solution.py:34
  9.3 0.0 collective-permute-done.3.r_ref
  9.3 0.0 copy-start.2
  9.3 0.0 copy-start.3
  9.3 0.6 shard_map.318
  9.9 0.0 collective-permute-done.2.r_ref
  9.9 0.0 copy-start
  10.0 0.0 copy-start.1
  10.0 0.0 copy-start.4
  10.0 0.0 copy-start.7
  10.0 0.0 copy-start.8
  10.0 0.0 copy-start.9
  10.0 0.6 %shard_map.319 = (f32[256,1408]{1,0:T(8,128)S(1)}, f32[48,128]{1,0:T(8,128)S(1)}) custom-call(f32[256,1408]{1,0:T(8,128)S(1)} %get-tuple-element.62.g_ref, f32[256,1408]{1,0:T(8,128)S(1)} %get-tuple-element.63.m_ref, f32[256,1408]{1,0:T(8,128)S(1)} %collective-permute-done.2.r_ref, ...), custom_call_target="tpu_custom_call", output_to_operand_aliasing={{1}: (3, {})} | custom-call | flops 1048576 | tf_op jit(solution)/shard_map/pallas_call | solution.py:34
  10.7 0.5 collective-permute-start.15
  11.1 0.1 collective-permute-start.14
  11.2 0.4 collective-permute-start.16
  11.7 0.1 collective-permute-start.1
  11.8 7.1 %collective-permute-done.1.r_ref = f32[256,512]{1,0:T(8,128)S(1)} collective-permute-done((f32[256,512]{1,0:T(8,128)S(1)}, f32[256,512]{1,0:T(8,128)S(1)}, u32[]{:S(2)}, u32[]{:S(2)}) %collective-permute-start.1) | collective-permute-done | bytes 524320 | tf_op jit(solution)/shard_map/ppermute | solution.py:47
  18.9 0.3 shard_map.320
  19.2 0.4 collective-permute-start.17
  19.6 2.6 %collective-permute-start.4 = (f32[16,128]{1,0:T(8,128)S(1)}, f32[16,128]{1,0:T(8,128)S(1)}, u32[]{:S(2)}, u32[]{:S(2)}) collective-permute-start(f32[16,128]{1,0:T(8,128)S(1)} %slice.3), channel_id=1, source_target_pairs={{0,2},{2,0},{4,6},{6,4},{1,3},{3,1},{5,7},{7,5},{8,10},{10,8},{12,... | collective-permute-start | bytes 24584 | tf_op jit(solution)/shard_map/ppermute | solution.py:428
  22.2 1.6 %collective-permute-done.4.refs_5_ = f32[16,128]{1,0:T(8,128)S(1)} collective-permute-done((f32[16,128]{1,0:T(8,128)S(1)}, f32[16,128]{1,0:T(8,128)S(1)}, u32[]{:S(2)}, u32[]{:S(2)}) %collective-permute-start.4) | collective-permute-done | bytes 8224 | tf_op jit(solution)/shard_map/ppermute | solution.py:428
  23.8 2.1 %collective-permute-start.5 = (f32[16,128]{1,0:T(8,128)S(1)}, f32[16,128]{1,0:T(8,128)S(1)}, u32[]{:S(2)}, u32[]{:S(2)}) collective-permute-start(f32[16,128]{1,0:T(8,128)S(1)} %slice.3), channel_id=1, source_target_pairs={{0,4},{2,6},{4,0},{6,2},{1,5},{3,7},{5,1},{7,3},{8,12},{10,14},{12... | collective-permute-start | bytes 24584 | tf_op jit(solution)/shard_map/ppermute | solution.py:428
  25.9 1.6 %collective-permute-done.5.refs_6_ = f32[16,128]{1,0:T(8,128)S(1)} collective-permute-done((f32[16,128]{1,0:T(8,128)S(1)}, f32[16,128]{1,0:T(8,128)S(1)}, u32[]{:S(2)}, u32[]{:S(2)}) %collective-permute-start.5) | collective-permute-done | bytes 8224 | tf_op jit(solution)/shard_map/ppermute | solution.py:428
  27.5 3.0 %collective-permute-start.6 = (f32[16,128]{1,0:T(8,128)S(1)}, f32[16,128]{1,0:T(8,128)S(1)}, u32[]{:S(2)}, u32[]{:S(2)}) collective-permute-start(f32[16,128]{1,0:T(8,128)S(1)} %slice.3), channel_id=1, source_target_pairs={{0,6},{2,4},{4,2},{6,0},{1,7},{3,5},{5,3},{7,1},{8,14},{10,12},{12... | collective-permute-start | bytes 24584 | tf_op jit(solution)/shard_map/ppermute | solution.py:428
  30.5 1.6 %collective-permute-done.6.refs_7_ = f32[16,128]{1,0:T(8,128)S(1)} collective-permute-done((f32[16,128]{1,0:T(8,128)S(1)}, f32[16,128]{1,0:T(8,128)S(1)}, u32[]{:S(2)}, u32[]{:S(2)}) %collective-permute-start.6) | collective-permute-done | bytes 8224 | tf_op jit(solution)/shard_map/ppermute | solution.py:428
  32.1 0.0 copy-done.2
  32.1 0.0 copy-done
  32.2 0.0 copy-start.5
  32.2 0.0 copy-start.6
  32.2 0.0 copy-start.10
  32.2 0.0 copy-start.11
  32.2 1.0 %shard_map.321 = (f32[16,128]{1,0:T(8,128)S(1)}, f32[1536,128]{1,0:T(8,128)S(1)}, f32[64,128]{1,0:T(8,128)S(1)}) custom-call(f32[4,128]{1,0:T(4,128)S(1)} %bitcast.19, f32[4,128]{1,0:T(4,128)S(1)} %bitcast.20, f32[11,128]{1,0:T(8,128)S(1)} %bitcast.16, f32[4,128]{1,0:T(4,128)S(1)} %bitcast.21, f32[48,128]{1,0:T(8,128)S(1)} %get-tuple-element.71.refs_4_, ...), custom_call_target="tpu_custom_call" | custom-call | flops 2097152 | tf_op jit(solution)/shard_map/pallas_call | solution.py:34
  33.2 2.1 %collective-permute-start.7 = (f32[64,128]{1,0:T(8,128)S(1)}, f32[64,128]{1,0:T(8,128)S(1)}, u32[]{:S(2)}, u32[]{:S(2)}) collective-permute-start(f32[64,128]{1,0:T(8,128)S(1)} %get-tuple-element.76.refs_4_), channel_id=1, source_target_pairs={{0,8},{8,0},{16,24},{24,16},{1,9},{9,1},{17,25},{25,17},{2,10},{10... | collective-permute-start | bytes 98312 | tf_op jit(solution)/shard_map/ppermute | solution.py:428
  35.4 2.2 %collective-permute-done.7 = f32[64,128]{1,0:T(8,128)S(1)} collective-permute-done((f32[64,128]{1,0:T(8,128)S(1)}, f32[64,128]{1,0:T(8,128)S(1)}, u32[]{:S(2)}, u32[]{:S(2)}) %collective-permute-start.7) | collective-permute-done | bytes 32800 | tf_op jit(solution)/shard_map/ppermute | solution.py:428
  37.6 2.7 %collective-permute-start.8 = (f32[64,128]{1,0:T(8,128)S(1)}, f32[64,128]{1,0:T(8,128)S(1)}, u32[]{:S(2)}, u32[]{:S(2)}) collective-permute-start(f32[64,128]{1,0:T(8,128)S(1)} %get-tuple-element.76.refs_4_), channel_id=1, source_target_pairs={{0,16},{8,24},{16,0},{24,8},{1,17},{9,25},{17,1},{25,9},{2,18},{10... | collective-permute-start | bytes 98312 | tf_op jit(solution)/shard_map/ppermute | solution.py:428
  40.3 2.2 %collective-permute-done.8 = f32[64,128]{1,0:T(8,128)S(1)} collective-permute-done((f32[64,128]{1,0:T(8,128)S(1)}, f32[64,128]{1,0:T(8,128)S(1)}, u32[]{:S(2)}, u32[]{:S(2)}) %collective-permute-start.8) | collective-permute-done | bytes 32800 | tf_op jit(solution)/shard_map/ppermute | solution.py:428
  42.5 3.9 %collective-permute-start.9 = (f32[64,128]{1,0:T(8,128)S(1)}, f32[64,128]{1,0:T(8,128)S(1)}, u32[]{:S(2)}, u32[]{:S(2)}) collective-permute-start(f32[64,128]{1,0:T(8,128)S(1)} %get-tuple-element.76.refs_4_), channel_id=1, source_target_pairs={{0,24},{8,16},{16,8},{24,0},{1,25},{9,17},{17,9},{25,1},{2,26},{10... | collective-permute-start | bytes 98312 | tf_op jit(solution)/shard_map/ppermute | solution.py:428
  46.4 1.9 %collective-permute-done.9 = f32[64,128]{1,0:T(8,128)S(1)} collective-permute-done((f32[64,128]{1,0:T(8,128)S(1)}, f32[64,128]{1,0:T(8,128)S(1)}, u32[]{:S(2)}, u32[]{:S(2)}) %collective-permute-start.9) | collective-permute-done | bytes 32800 | tf_op jit(solution)/shard_map/ppermute | solution.py:428
  48.3 0.1 collective-permute-start.10
  48.4 1.2 %collective-permute-done.10.other_ref = f32[64,128]{1,0:T(8,128)S(1)} collective-permute-done((f32[64,128]{1,0:T(8,128)S(1)}, f32[64,128]{1,0:T(8,128)S(1)}, u32[]{:S(2)}, u32[]{:S(2)}) %collective-permute-start.10) | collective-permute-done | bytes 32800 | tf_op jit(solution)/shard_map/ppermute | solution.py:47
  49.6 0.2 collective-permute-start.18
  49.7 0.0 copy-done.11
  49.7 0.1 shard_map.322
  49.9 0.8 %collective-permute-done.18.refs_9_ = f32[16,128]{1,0:T(8,128)S(1)} collective-permute-done((f32[16,128]{1,0:T(8,128)S(1)}, f32[16,128]{1,0:T(8,128)S(1)}, u32[]{:S(2)}, u32[]{:S(2)}) %collective-permute-start.18) | collective-permute-done | bytes 8224 | tf_op jit(solution)/shard_map/ppermute | solution.py:47
  50.7 1.5 %collective-permute-start.11 = (f32[8,128]{1,0:T(8,128)S(1)}, f32[8,128]{1,0:T(8,128)S(1)}, u32[]{:S(2)}, u32[]{:S(2)}) collective-permute-start(f32[8,128]{1,0:T(8,128)S(1)} %get-tuple-element.77.refs_0_), channel_id=1, source_target_pairs={{0,2},{2,0},{4,6},{6,4},{1,3},{3,1},{5,7},{7,5},{8,10},{10,8},{12,... | collective-permute-start | bytes 12296 | tf_op jit(solution)/shard_map/ppermute | solution.py:428
  52.2 0.0 collective-permute-done.17.refs_3_.refs_14_
  52.2 1.5 %collective-permute-start.12 = (f32[8,128]{1,0:T(8,128)S(1)}, f32[8,128]{1,0:T(8,128)S(1)}, u32[]{:S(2)}, u32[]{:S(2)}) collective-permute-start(f32[8,128]{1,0:T(8,128)S(1)} %get-tuple-element.77.refs_0_), channel_id=1, source_target_pairs={{0,4},{2,6},{4,0},{6,2},{1,5},{3,7},{5,1},{7,3},{8,12},{10,14},{12... | collective-permute-start | bytes 12296 | tf_op jit(solution)/shard_map/ppermute | solution.py:428
  53.8 0.0 collective-permute-done.15.refs_1_.refs_12_
  53.8 0.5 collective-permute-start.13
  54.2 2.2 %shard_map.323 = (f32[512,1408]{1,0:T(8,128)}, f32[512,1408]{1,0:T(8,128)}, f32[1408,512]{1,0:T(8,128)}, f32[512,512]{1,0:T(8,128)}) custom-call(f32[256,1408]{1,0:T(8,128)S(1)} %get-tuple-element.72.refs_8_.refs_0_.refs_7_, f32[256,1408]{1,0:T(8,128)S(1)} %get-tuple-element.73.refs_9_.refs_1_.refs_8_, ...), custom_call_target="tpu_custom_call" | custom-call | flops 16777216 | tf_op jit(solution)/shard_map/pallas_call | solution.py:34
  56.5 0.0 collective-permute-done.14.refs_0_.refs_11_
  56.5 0.0 collective-permute-done.16.refs_2_.refs_13_
  56.5 2.4 %shard_map.324 = (f32[512,1408]{1,0:T(8,128)}, f32[512,1408]{1,0:T(8,128)}, f32[1408,512]{1,0:T(8,128)}, f32[512,512]{1,0:T(8,128)}, f32[4,128]{1,0:T(4,128)}, /...) custom-call(f32[256,1408]{1,0:T(8,128)S(1)} %collective-permute-done, ...), custom_call_target="tpu_custom_call", output_to_operand_aliasing={{0}: (4, {}), {1}: (5, {}), {2}: (6, {}), {3}: (7, {})} | custom-call | flops 16777216 | tf_op jit(solution)/shard_map/pallas_call | solution.py:34
  58.9 0.0 collective-permute-done.11.refs_1_
  58.9 0.0 collective-permute-done.12.refs_2_
  58.9 0.0 collective-permute-done.13.refs_3_
  58.9 4.1 %shard_map.325 = (f32[512,1408]{1,0:T(8,128)}, f32[512,1408]{1,0:T(8,128)}, f32[1408,512]{1,0:T(8,128)}, f32[512,512]{1,0:T(8,128)}) custom-call(f32[8,128]{1,0:T(8,128)S(1)} %get-tuple-element.77.refs_0_, f32[8,128]{1,0:T(8,128)S(1)} %collective-permute-done.11.refs_1_, f32[8,128]{1,0:T(8,128)S(1)} %collective-permute-done.12.refs_2_, ...), custom_call_target="tpu_custom_call" | custom-call | flops 4194304 | tf_op jit(solution)/shard_map/pallas_call | solution.py:34
  (11 shorter events, 0.0 us)
Async XLA Ops:
  2.0 3.4 %collective-permute-start = (f32[704,512]{1,0:T(8,128)S(1)}, f32[704,512]{1,0:T(8,128)S(1)}, u32[]{:S(2)}, u32[]{:S(2)}) collective-permute-start(f32[704,512]{1,0:T(8,128)S(1)} %shard_map.315), channel_id=1, source_target_pairs={{0,1},{1,0},{2,3},{3,2},{4,5},{5,4},{6,7},{7,6},{8,9},{9,8},{10,11... | collective-permute-start | bytes 4325384 | tf_op jit(solution)/shard_map/ppermute | solution.py:47
  4.5 4.8 %collective-permute-start.3 = (f32[256,1408]{1,0:T(8,128)S(1)}, f32[256,1408]{1,0:T(8,128)S(1)}, u32[]{:S(2)}, u32[]{:S(2)}) collective-permute-start(f32[256,1408]{1,0:T(8,128)S(1)} %get-tuple-element.67), channel_id=1, source_target_pairs={{0,1},{1,0},{2,3},{3,2},{4,5},{5,4},{6,7},{7,6},{8,9},{9,8},{10,11... | collective-permute-start | bytes 4325384 | tf_op jit(solution)/shard_map/ppermute | solution.py:47
  4.6 5.3 %collective-permute-start.2 = (f32[256,1408]{1,0:T(8,128)S(1)}, f32[256,1408]{1,0:T(8,128)S(1)}, u32[]{:S(2)}, u32[]{:S(2)}) collective-permute-start(f32[256,1408]{1,0:T(8,128)S(1)} %get-tuple-element.64), channel_id=1, source_target_pairs={{0,1},{1,0},{2,3},{3,2},{4,5},{5,4},{6,7},{7,6},{8,9},{9,8},{10,11... | collective-permute-start | bytes 4325384 | tf_op jit(solution)/shard_map/ppermute | solution.py:47
  9.3 22.8 %copy-start.2 = (f32[1408,512]{1,0:T(8,128)S(1)}, f32[1408,512]{1,0:T(8,128)}, u32[]{:S(2)}) copy-start(f32[1408,512]{1,0:T(8,128)} %refs_17_.1) | copy-start | bytes 8650756
  9.3 22.8 %copy-start.3 = (f32[512,512]{1,0:T(8,128)S(1)}, f32[512,512]{1,0:T(8,128)}, u32[]{:S(2)}) copy-start(f32[512,512]{1,0:T(8,128)} %refs_18_.1) | copy-start | bytes 3145732
  9.9 22.2 %copy-start = (f32[512,1408]{1,0:T(8,128)S(1)}, f32[512,1408]{1,0:T(8,128)}, u32[]{:S(2)}) copy-start(f32[512,1408]{1,0:T(8,128)} %refs_15_.3) | copy-start | bytes 8650756
  10.0 22.1 %copy-start.1 = (f32[512,1408]{1,0:T(8,128)S(1)}, f32[512,1408]{1,0:T(8,128)}, u32[]{:S(2)}) copy-start(f32[512,1408]{1,0:T(8,128)} %refs_16_.1) | copy-start | bytes 8650756
  10.0 22.1 %copy-start.4 = (f32[1408]{0:T(1024)S(1)}, f32[1408]{0:T(1024)}, u32[]{:S(2)}) copy-start(f32[1408]{0:T(1024)} %param.33) | copy-start | bytes 16900
  10.0 22.1 %copy-start.7 = (f32[512]{0:T(512)S(1)}, f32[512]{0:T(512)}, u32[]{:S(2)}) copy-start(f32[512]{0:T(512)} %param.23) | copy-start | bytes 6148
  10.0 22.1 %copy-start.8 = (f32[512]{0:T(512)S(1)}, f32[512]{0:T(512)}, u32[]{:S(2)}) copy-start(f32[512]{0:T(512)} %param.28) | copy-start | bytes 6148
  10.0 22.1 %copy-start.9 = (f32[512]{0:T(512)S(1)}, f32[512]{0:T(512)}, u32[]{:S(2)}) copy-start(f32[512]{0:T(512)} %param.38) | copy-start | bytes 6148
  10.7 43.1 %collective-permute-start.15 = (f32[256,1408]{1,0:T(8,128)S(1)}, f32[256,1408]{1,0:T(8,128)S(1)}, u32[]{:S(2)}, u32[]{:S(2)}) collective-permute-start(f32[256,1408]{1,0:T(8,128)S(1)} %get-tuple-element.73.refs_9_.refs_1_.refs_8_), channel_id=1, source_target_pairs={{0,1},{1,0},{2,3},{3,2},{4,5},{5,4},{6,7},{7,6},{8,9},{9,8},{10,11... | collective-permute-start | bytes 4325384 | tf_op jit(solution)/shard_map/ppermute | solution.py:47
  11.1 45.3 %collective-permute-start.14 = (f32[256,1408]{1,0:T(8,128)S(1)}, f32[256,1408]{1,0:T(8,128)S(1)}, u32[]{:S(2)}, u32[]{:S(2)}) collective-permute-start(f32[256,1408]{1,0:T(8,128)S(1)} %get-tuple-element.72.refs_8_.refs_0_.refs_7_), channel_id=1, source_target_pairs={{0,1},{1,0},{2,3},{3,2},{4,5},{5,4},{6,7},{7,6},{8,9},{9,8},{10,11... | collective-permute-start | bytes 4325384 | tf_op jit(solution)/shard_map/ppermute | solution.py:47
  11.2 45.3 %collective-permute-start.16 = (f32[704,512]{1,0:T(8,128)S(1)}, f32[704,512]{1,0:T(8,128)S(1)}, u32[]{:S(2)}, u32[]{:S(2)}) collective-permute-start(f32[704,512]{1,0:T(8,128)S(1)} %get-tuple-element.74.refs_10_.refs_2_.refs_9_), channel_id=1, source_target_pairs={{0,1},{1,0},{2,3},{3,2},{4,5},{5,4},{6,7},{7,6},{8,9},{9,8},{10,11... | collective-permute-start | bytes 4325384 | tf_op jit(solution)/shard_map/ppermute | solution.py:47
  11.7 7.2 %collective-permute-start.1 = (f32[256,512]{1,0:T(8,128)S(1)}, f32[256,512]{1,0:T(8,128)S(1)}, u32[]{:S(2)}, u32[]{:S(2)}) collective-permute-start(f32[256,512]{1,0:T(8,128)S(1)} %get-tuple-element.61), channel_id=1, source_target_pairs={{0,1},{1,0},{2,3},{3,2},{4,5},{5,4},{6,7},{7,6},{8,9},{9,8},{10,11... | collective-permute-start | bytes 1572872 | tf_op jit(solution)/shard_map/ppermute | solution.py:47
  19.2 33.1 %collective-permute-start.17 = (f32[256,512]{1,0:T(8,128)S(1)}, f32[256,512]{1,0:T(8,128)S(1)}, u32[]{:S(2)}, u32[]{:S(2)}) collective-permute-start(f32[256,512]{1,0:T(8,128)S(1)} %get-tuple-element.75.refs_11_.refs_3_.refs_10_), channel_id=1, source_target_pairs={{0,1},{1,0},{2,3},{3,2},{4,5},{5,4},{6,7},{7,6},{8,9},{9,8},{10,11... | collective-permute-start | bytes 1572872 | tf_op jit(solution)/shard_map/ppermute | solution.py:47
  19.6 4.2 %collective-permute-start.4 = (f32[16,128]{1,0:T(8,128)S(1)}, f32[16,128]{1,0:T(8,128)S(1)}, u32[]{:S(2)}, u32[]{:S(2)}) collective-permute-start(f32[16,128]{1,0:T(8,128)S(1)} %slice.3), channel_id=1, source_target_pairs={{0,2},{2,0},{4,6},{6,4},{1,3},{3,1},{5,7},{7,5},{8,10},{10,8},{12,... | collective-permute-start | bytes 24584 | tf_op jit(solution)/shard_map/ppermute | solution.py:428
  23.8 3.7 %collective-permute-start.5 = (f32[16,128]{1,0:T(8,128)S(1)}, f32[16,128]{1,0:T(8,128)S(1)}, u32[]{:S(2)}, u32[]{:S(2)}) collective-permute-start(f32[16,128]{1,0:T(8,128)S(1)} %slice.3), channel_id=1, source_target_pairs={{0,4},{2,6},{4,0},{6,2},{1,5},{3,7},{5,1},{7,3},{8,12},{10,14},{12... | collective-permute-start | bytes 24584 | tf_op jit(solution)/shard_map/ppermute | solution.py:428
  27.5 4.6 %collective-permute-start.6 = (f32[16,128]{1,0:T(8,128)S(1)}, f32[16,128]{1,0:T(8,128)S(1)}, u32[]{:S(2)}, u32[]{:S(2)}) collective-permute-start(f32[16,128]{1,0:T(8,128)S(1)} %slice.3), channel_id=1, source_target_pairs={{0,6},{2,4},{4,2},{6,0},{1,7},{3,5},{5,3},{7,1},{8,14},{10,12},{12... | collective-permute-start | bytes 24584 | tf_op jit(solution)/shard_map/ppermute | solution.py:428
  32.2 17.6 %copy-start.5 = (f32[1408]{0:T(1024)S(1)}, f32[1408]{0:T(1024)}, u32[]{:S(2)}) copy-start(f32[1408]{0:T(1024)} %param.24) | copy-start | bytes 16900
  32.2 17.6 %copy-start.6 = (f32[1408]{0:T(1024)S(1)}, f32[1408]{0:T(1024)}, u32[]{:S(2)}) copy-start(f32[1408]{0:T(1024)} %param.29) | copy-start | bytes 16900
  32.2 17.6 %copy-start.10 = (f32[512]{0:T(512)S(1)}, f32[512]{0:T(512)}, u32[]{:S(2)}) copy-start(f32[512]{0:T(512)} %param.34) | copy-start | bytes 6148
  32.2 17.5 %copy-start.11 = (f32[512]{0:T(512)S(1)}, f32[512]{0:T(512)}, u32[]{:S(2)}) copy-start(f32[512]{0:T(512)} %param.39) | copy-start | bytes 6148
  33.2 4.3 %collective-permute-start.7 = (f32[64,128]{1,0:T(8,128)S(1)}, f32[64,128]{1,0:T(8,128)S(1)}, u32[]{:S(2)}, u32[]{:S(2)}) collective-permute-start(f32[64,128]{1,0:T(8,128)S(1)} %get-tuple-element.76.refs_4_), channel_id=1, source_target_pairs={{0,8},{8,0},{16,24},{24,16},{1,9},{9,1},{17,25},{25,17},{2,10},{10... | collective-permute-start | bytes 98312 | tf_op jit(solution)/shard_map/ppermute | solution.py:428
  37.6 4.9 %collective-permute-start.8 = (f32[64,128]{1,0:T(8,128)S(1)}, f32[64,128]{1,0:T(8,128)S(1)}, u32[]{:S(2)}, u32[]{:S(2)}) collective-permute-start(f32[64,128]{1,0:T(8,128)S(1)} %get-tuple-element.76.refs_4_), channel_id=1, source_target_pairs={{0,16},{8,24},{16,0},{24,8},{1,17},{9,25},{17,1},{25,9},{2,18},{10... | collective-permute-start | bytes 98312 | tf_op jit(solution)/shard_map/ppermute | solution.py:428
  42.5 5.8 %collective-permute-start.9 = (f32[64,128]{1,0:T(8,128)S(1)}, f32[64,128]{1,0:T(8,128)S(1)}, u32[]{:S(2)}, u32[]{:S(2)}) collective-permute-start(f32[64,128]{1,0:T(8,128)S(1)} %get-tuple-element.76.refs_4_), channel_id=1, source_target_pairs={{0,24},{8,16},{16,8},{24,0},{1,25},{9,17},{17,9},{25,1},{2,26},{10... | collective-permute-start | bytes 98312 | tf_op jit(solution)/shard_map/ppermute | solution.py:428
  48.3 1.3 %collective-permute-start.10 = (f32[64,128]{1,0:T(8,128)S(1)}, f32[64,128]{1,0:T(8,128)S(1)}, u32[]{:S(2)}, u32[]{:S(2)}) collective-permute-start(f32[64,128]{1,0:T(8,128)S(1)} %add_add_fusion.total_ref), channel_id=1, source_target_pairs={{0,1},{1,0},{2,3},{3,2},{4,5},{5,4},{6,7},{7,6},{8,9},{9,8},{10,11... | collective-permute-start | bytes 98312 | tf_op jit(solution)/shard_map/ppermute | solution.py:47
  49.6 1.2 %collective-permute-start.18 = (f32[16,128]{1,0:T(8,128)S(1)}, f32[16,128]{1,0:T(8,128)S(1)}, u32[]{:S(2)}, u32[]{:S(2)}) collective-permute-start(f32[16,128]{1,0:T(8,128)S(1)} %get-tuple-element.83.refs_8_), channel_id=1, source_target_pairs={{0,1},{1,0},{2,3},{3,2},{4,5},{5,4},{6,7},{7,6},{8,9},{9,8},{10,11... | collective-permute-start | bytes 24584 | tf_op jit(solution)/shard_map/ppermute | solution.py:47
  50.7 8.1 %collective-permute-start.11 = (f32[8,128]{1,0:T(8,128)S(1)}, f32[8,128]{1,0:T(8,128)S(1)}, u32[]{:S(2)}, u32[]{:S(2)}) collective-permute-start(f32[8,128]{1,0:T(8,128)S(1)} %get-tuple-element.77.refs_0_), channel_id=1, source_target_pairs={{0,2},{2,0},{4,6},{6,4},{1,3},{3,1},{5,7},{7,5},{8,10},{10,8},{12,... | collective-permute-start | bytes 12296 | tf_op jit(solution)/shard_map/ppermute | solution.py:428
  52.2 6.7 %collective-permute-start.12 = (f32[8,128]{1,0:T(8,128)S(1)}, f32[8,128]{1,0:T(8,128)S(1)}, u32[]{:S(2)}, u32[]{:S(2)}) collective-permute-start(f32[8,128]{1,0:T(8,128)S(1)} %get-tuple-element.77.refs_0_), channel_id=1, source_target_pairs={{0,4},{2,6},{4,0},{6,2},{1,5},{3,7},{5,1},{7,3},{8,12},{10,14},{12... | collective-permute-start | bytes 12296 | tf_op jit(solution)/shard_map/ppermute | solution.py:428
  53.8 5.1 %collective-permute-start.13 = (f32[8,128]{1,0:T(8,128)S(1)}, f32[8,128]{1,0:T(8,128)S(1)}, u32[]{:S(2)}, u32[]{:S(2)}) collective-permute-start(f32[8,128]{1,0:T(8,128)S(1)} %get-tuple-element.77.refs_0_), channel_id=1, source_target_pairs={{0,6},{2,4},{4,2},{6,0},{1,7},{3,5},{5,3},{7,1},{8,14},{10,12},{12... | collective-permute-start | bytes 12296 | tf_op jit(solution)/shard_map/ppermute | solution.py:428
